TPU v7x, 512 devices: a whole 4x8x8 slice. The times are simulated.
512 devices in a mesh: ep: 128 (over z, y, core), tp: 4 (over x).
Axes of the slice: x: 4, y: 8, z: 8, core: 2. Of those that a mesh axis runs over, the one named last changes fastest.
Arguments:
- tokens: bfloat16 [16384, 2048], P('ep'), may hold values from -6 to 6
- norm_gain: float32 [2048], replicated, may hold values from 0.1 to 1.9
- routes: int32 [16384, 2], P('ep'), may hold values from 0 to 31, as said below
- route_scores: float32 [16384, 2], P('ep'), may hold values from -6 to 6
- expert_gate: bfloat16 [128, 2048, 1024], P('ep', None, 'tp'), may hold values from -0.125 to 0.125
- expert_up: bfloat16 [128, 2048, 1024], P('ep', None, 'tp'), may hold values from -0.125 to 0.125
- expert_down: bfloat16 [128, 1024, 2048], P('ep', None, 'tp'), may hold values from -0.09375 to 0.09375
- branch_in: bfloat16 [2048, 512], P('ep', 'tp'), may hold values from -0.125 to 0.125
- branch_out: bfloat16 [512, 2048], P('tp', 'ep'), may hold values from -0.25 to 0.25
- branch_gate: float32 [2048], replicated, may hold values from -0.125 to 0.125
Outputs:
- mixed: bfloat16 [16384, 2048], P('ep', 'tp')
Inputs may be any that keep to these rules, and one draw needn't show every extreme that they name: `routes`: each row names 2 different experts. In each aligned block of 128 rows (the rows of one index of ep) no expert is named more than 10 times, and one expert, the same in every block, is named exactly 10 times in every block.
All inputs are finite; a program needn't handle non-finite values.
Results may differ from a plain program's by a relative error of at most 0.0066.
Values may be sent and summed in bfloat16 or wider, within the bound.
A program may use at most 64 MiB of HBM per device.

v0:
```python
import jax
import jax.numpy as jnp
from jax import lax
from jax.sharding import PartitionSpec as P

NORM_EPSILON = 1e-06


def joined_along(parts, dim):
    parts = jnp.moveaxis(parts, 0, dim)
    lengths = parts.shape
    return parts.reshape(*lengths[:dim], lengths[dim] * lengths[dim + 1], *lengths[dim + 2 :])


def copy_for_each(x, axis):
    size = lax.axis_size(axis)
    return lax.all_to_all(jnp.broadcast_to(x[None], (size, *x.shape)), axis, 0, 0, tiled=True)


def collect(x, axis, dim):
    return joined_along(copy_for_each(x, axis), dim)


def items_in_groups(x, axis, split_dim, concat_dim, work, item_dim, out_dim):

    def moved(group):
        return lax.all_to_all(group, axis, split_axis=split_dim, concat_axis=concat_dim, tiled=True)

    items = jax.tree.leaves(x)[0].shape[item_dim]
    ends = [items * k // 2 for k in range(2 + 1)] if items % 2 == 0 else [0, items]
    groups = [
        jax.tree.map(lambda a: lax.slice_in_dim(a, low, high, axis=item_dim), x)
        for low, high in zip(ends, ends[1:])
    ]
    arrived = [moved(group) for group in groups]
    made = [work(group) for group in arrived]
    return jax.tree.map(lambda *parts: jnp.concatenate(parts, axis=out_dim), *made)


def in_blocks(x, dim, size):
    before, after = (x.shape[:dim], x.shape[dim + 1 :])
    return jnp.moveaxis(x.reshape(*before, size, -1, *after), dim, 0)


def sent_and_summed(x, axis, dim):
    parts = in_blocks(x, dim, lax.axis_size(axis))
    arrived = lax.all_to_all(parts, axis, split_axis=0, concat_axis=0, tiled=True)
    return arrived.astype(jnp.float32).sum(axis=0)


def on_device(
    tokens,
    norm_gain,
    routes,
    route_scores,
    expert_gate,
    expert_up,
    expert_down,
    branch_in,
    branch_out,
    branch_gate,
):
    ep_count = lax.axis_size("ep")
    tp_count = lax.axis_size("tp")
    tok_rows = tokens.shape[0]
    model_width = tokens.shape[1]
    fanout = routes.shape[1]
    group_size = max(1, ep_count // 32)
    expert_count = ep_count // group_size
    capacity = 5 * tok_rows * fanout // (4 * expert_count)
    tokens_float = tokens.astype(jnp.float32)
    scaled = lax.rsqrt(jnp.mean(tokens_float * tokens_float, axis=-1, keepdims=True) + NORM_EPSILON)
    normed = (tokens_float * scaled * norm_gain).astype(jnp.bfloat16)
    flat_ids = routes.reshape(-1)
    choose = (flat_ids[:, None] == jnp.arange(expert_count, dtype=jnp.int32)[None, :]).astype(
        jnp.int32
    )
    earlier = jnp.cumsum(choose, axis=0, dtype=jnp.int32) - choose
    slot_index = jnp.sum(earlier * choose, axis=1, dtype=jnp.int32)
    position = flat_ids * capacity + slot_index
    owner_token = jnp.arange(tok_rows * fanout, dtype=jnp.int32) // fanout
    source_row = jnp.zeros((expert_count * capacity,), jnp.int32).at[position].set(owner_token)
    filled = jnp.zeros((expert_count * capacity,), jnp.bool_).at[position].set(True)
    packed = jnp.where(filled[:, None], normed[source_row], jnp.zeros((), jnp.bfloat16))
    w_gate = expert_gate[0]
    w_up = expert_up[0]
    w_down = expert_down[0]

    def finish(gate_pre, up_pre, slot_count):
        hidden = (jax.nn.silu(gate_pre) * up_pre).astype(jnp.bfloat16)
        start_sum = jnp.zeros((hidden.shape[0], w_down.shape[1]), jnp.float32)
        partial_out = start_sum + jnp.dot(
            collect(hidden, "tp", 1), w_down, preferred_element_type=jnp.float32
        )
        partial_out = partial_out.reshape(ep_count, slot_count, w_down.shape[1])
        return lax.all_to_all(
            partial_out.astype(jnp.bfloat16), "ep", split_axis=0, concat_axis=0, tiled=True
        ).astype(partial_out.dtype)

    column_width = model_width // tp_count
    own_columns = lax.dynamic_slice_in_dim(
        packed, lax.axis_index("tp") * column_width, column_width, 1
    )
    outgoing = jnp.broadcast_to(
        own_columns.reshape(expert_count, 1, capacity, column_width),
        (expert_count, group_size, capacity, column_width),
    ).reshape(ep_count, capacity, column_width)

    def expert_columns(arrived):
        slot_count = arrived.shape[1]
        flat_rows = arrived.reshape(ep_count * slot_count, column_width)
        start_zero = jnp.zeros((flat_rows.shape[0], w_gate.shape[1]), jnp.float32)
        part_rows = lax.all_gather(flat_rows, "tp", axis=1, tiled=True)
        gate_pre = start_zero + jnp.dot(part_rows, w_gate, preferred_element_type=jnp.float32)
        up_pre = start_zero + jnp.dot(part_rows, w_up, preferred_element_type=jnp.float32)
        return finish(gate_pre, up_pre, slot_count)

    returned = items_in_groups(outgoing, "ep", 0, 0, expert_columns, 1, 1)
    per_slot = jnp.sum(returned.reshape(expert_count, group_size, capacity, -1), axis=1)
    per_slot = per_slot.reshape(expert_count * capacity, -1)
    difference = route_scores[:, 0] - route_scores[:, 1]
    route_weight = jnp.stack(
        [jax.nn.sigmoid(difference), jax.nn.sigmoid(-difference)], axis=1
    ).reshape(-1)
    routed = jnp.sum(
        (per_slot[position] * route_weight[:, None]).reshape(tok_rows, fanout, -1), axis=1
    )
    whole_in = lax.all_gather(branch_in, "ep", axis=0, tiled=True)
    branch_pre = jnp.dot(normed, whole_in, preferred_element_type=jnp.float32)
    branch_hidden = jax.nn.silu(branch_pre).astype(jnp.bfloat16)
    whole_out = lax.all_gather(branch_out, "ep", axis=1, tiled=True)
    branch_terms = jnp.dot(branch_hidden, whole_out, preferred_element_type=jnp.float32)
    branch_share = sent_and_summed(branch_terms.astype(jnp.bfloat16), "tp", 1)
    branch_weight = jax.nn.sigmoid(jnp.sum(normed.astype(jnp.float32) * branch_gate, axis=-1))
    return (routed + branch_weight[:, None] * branch_share).astype(jnp.bfloat16)


def solution(mesh):
    in_specs = (
        P("ep", None),
        P(),
        P("ep", None),
        P("ep", None),
        P("ep", None, "tp"),
        P("ep", None, "tp"),
        P("ep", None, "tp"),
        P("ep", "tp"),
        P("tp", "ep"),
        P(),
    )
    out_specs = P("ep", "tp")
    return jax.shard_map(
        on_device, mesh=mesh, in_specs=in_specs, out_specs=out_specs, check_vma=False
    )
```

profile of v0, /device:TPU:1, one launch (start us, length us, event | category | flops | bytes accessed | tf_op | source)
XLA Modules:
  0.0 355.5 jit_solution(6448514698254923518)
XLA Ops:
  9.6 1.4 scatter_custom_fusion.1
  12.3 1.4 multiply_reduce_fusion
  13.7 2.4 gather_fusion
  16.1 1.5 scatter_custom_fusion
  18.1 1.4 fusion.26
  19.6 49.2 %all_to_all.35 = bf16[128,5,512]{2,1,0:T(8,128)(2,1)S(1)} all-to-all(bf16[128,5,512]{2,1,0:T(8,128)(2,1)S(1)} %get-tuple-element.7), channel_id=1, replica_groups=mesh['ep'=128,'tp'=4] {'ep'}, dimensions={0} | all-to-all | bytes 1310720 | tf_op jit(solution)/shard_map/all_to_all | solution.py:27
  69.9 37.4 %all_to_all.36 = bf16[128,5,512]{2,1,0:T(8,128)(2,1)S(1)} all-to-all(bf16[128,5,512]{2,1,0:T(8,128)(2,1)} %get-tuple-element.8), channel_id=1, replica_groups=mesh['ep'=128,'tp'=4] {'ep'}, dimensions={0} | all-to-all | bytes 1310720 | tf_op jit(solution)/shard_map/all_to_all | solution.py:27
  108.5 49.6 %all_gather.14 = bf16[2048,128]{1,0:T(8,128)(2,1)S(1)} all-gather(bf16[16,128]{1,0:T(8,128)(2,1)S(1)} %copy-done.2), channel_id=1, replica_groups=mesh['ep'=128,'tp'=4] {'ep'}, dimensions={0}, use_global_device_ids=true | all-gather | bytes 528384 | tf_op jit(solution)/shard_map/all_gather | solution.py:128
  158.1 48.7 %all_gather.15 = bf16[128,2048]{0,1:T(8,128)(2,1)S(1)} all-gather(bf16[128,16]{0,1:T(8,128)(2,1)S(1)} %copy-done.3), channel_id=1, replica_groups=mesh['ep'=128,'tp'=4] {'ep'}, dimensions={1}, use_global_device_ids=true | all-gather | bytes 528384 | tf_op jit(solution)/shard_map/all_gather | solution.py:131
  208.1 4.0 %all-to-all-start.6 = ((bf16[4,128,512]{2,1,0:T(8,128)(2,1)}), bf16[4,128,512]{2,1,0:T(8,128)(2,1)S(1)}, u32[]{:S(2)}, u32[]{:S(2)}) async-start(bf16[4,128,512]{2,1,0:T(8,128)(2,1)} %bitcast.56), calls=%async_computation.6 | async-start | bytes 1048576 | tf_op jit(solution)/shard_map/all_to_all | solution.py:47
  212.2 2.7 fusion.13
  215.8 5.5 %all-to-all-done.6 = bf16[4,128,512]{2,1,0:T(8,128)(2,1)S(1)} async-done(((bf16[4,128,512]{2,1,0:T(8,128)(2,1)}), bf16[4,128,512]{2,1,0:T(8,128)(2,1)S(1)}, u32[]{:S(2)}, u32[]{:S(2)}) %all-to-all-start.6) | async-done | bytes 524320 | tf_op jit(solution)/shard_map/all_to_all | solution.py:47
  221.3 1.2 broadcast_in_dim.56
  222.5 3.5 all-to-all-start.1
  226.1 2.7 fusion.11
  229.7 13.0 %all-to-all-done.1 = bf16[4,640,256]{2,1,0:T(8,128)(2,1)S(1)} async-done(((bf16[4,640,256]{2,1,0:T(8,128)(2,1)}), bf16[4,640,256]{2,1,0:T(8,128)(2,1)S(1)}, u32[]{:S(2)}, u32[]{:S(2)}) %all-to-all-start.1) | async-done | bytes 1310752 | tf_op jit(solution)/shard_map/all_to_all | solution.py:17
  243.9 4.3 %all-to-all-start.4 = ((bf16[4,640,256]{2,1,0:T(8,128)(2,1)}), bf16[4,640,256]{2,1,0:T(8,128)(2,1)}, u32[]{:S(2)}, u32[]{:S(2)}) async-start(bf16[4,640,256]{2,1,0:T(8,128)(2,1)} %broadcast_in_dim.57), calls=%async_computation.4 | async-start | bytes 2621440 | tf_op jit(solution)/shard_map/all_to_all | solution.py:17
  248.2 2.1 copy.23
  250.3 3.0 dot_general.30
  253.3 1.5 convolution_convert_fusion.2
  254.8 1.4 copy.25
  256.2 7.9 %all-to-all-done.4 = bf16[4,640,256]{2,1,0:T(8,128)(2,1)} async-done(((bf16[4,640,256]{2,1,0:T(8,128)(2,1)}), bf16[4,640,256]{2,1,0:T(8,128)(2,1)}, u32[]{:S(2)}, u32[]{:S(2)}) %all-to-all-start.4) | async-done | bytes 1310752 | tf_op jit(solution)/shard_map/all_to_all | solution.py:17
  264.1 10.3 %all-to-all-start.2 = ((bf16[128,5,512]{2,1,0:T(8,128)(2,1)}), bf16[128,5,512]{2,1,0:T(8,128)(2,1)S(1)}, u32[]{:S(2)}, u32[]{:S(2)}) async-start(bf16[128,5,512]{2,1,0:T(8,128)(2,1)} %copy.25), calls=%async_computation.2 | async-start | bytes 2097152 | tf_op jit(solution)/shard_map/all_to_all | solution.py:96
  274.4 2.3 copy.26
  276.7 2.0 dot_general.34
  278.7 3.1 convolution_convert_fusion.1
  281.8 1.4 copy.28
  283.2 22.1 %all-to-all-done.2 = bf16[128,5,512]{2,1,0:T(8,128)(2,1)S(1)} async-done(((bf16[128,5,512]{2,1,0:T(8,128)(2,1)}), bf16[128,5,512]{2,1,0:T(8,128)(2,1)S(1)}, u32[]{:S(2)}, u32[]{:S(2)}) %all-to-all-start.2) | async-done | bytes 655392 | tf_op jit(solution)/shard_map/all_to_all | solution.py:96
  305.3 6.4 %all-to-all-start.5 = ((bf16[128,5,512]{2,1,0:T(8,128)(2,1)}), bf16[128,5,512]{2,1,0:T(8,128)(2,1)S(1)}, u32[]{:S(2)}, u32[]{:S(2)}) async-start(bf16[128,5,512]{2,1,0:T(8,128)(2,1)} %copy.28), calls=%async_computation.5 | async-start | bytes 2097152 | tf_op jit(solution)/shard_map/all_to_all | solution.py:96
  313.1 29.6 %all-to-all-done.5 = bf16[128,5,512]{2,1,0:T(8,128)(2,1)S(1)} async-done(((bf16[128,5,512]{2,1,0:T(8,128)(2,1)}), bf16[128,5,512]{2,1,0:T(8,128)(2,1)S(1)}, u32[]{:S(2)}, u32[]{:S(2)}) %all-to-all-start.5) | async-done | bytes 655392 | tf_op jit(solution)/shard_map/all_to_all | solution.py:96
  342.7 1.8 convert_reduce_fusion
  344.6 1.3 reshape.110
  (65 shorter events, 15.5 us)
Async XLA Ops:
  6.5 246.7 %copy-start = (bf16[1,1024,512]{2,1,0:T(8,128)(2,1)S(1)}, bf16[1,1024,512]{2,1,0:T(8,128)(2,1)}, u32[]{:S(2)}) copy-start(bf16[1,1024,512]{2,1,0:T(8,128)(2,1)} %param.16) | copy-start | bytes 3145732
  6.5 205.6 %all-gather.3.cloned.1.call-start = ((), (), s32[]{:S(2)}) async-start(), calls=%async_computation.7 | async-start | bytes 3276800 | tf_op jit(solution)/shard_map/all_gather | solution.py:113
  69.9 156.2 %all-gather.5.cloned.1.call-start = ((), (), s32[]{:S(2)}) async-start(), calls=%async_computation.8 | async-start | bytes 3276800 | tf_op jit(solution)/shard_map/all_gather | solution.py:113
  69.9 38.6 %copy-start.2 = (bf16[16,128]{1,0:T(8,128)(2,1)S(1)}, bf16[16,128]{1,0:T(8,128)(2,1)}, u32[]{:S(2)}) copy-start(bf16[16,128]{1,0:T(8,128)(2,1)} %param.17) | copy-start | bytes 12292
  69.9 88.1 %copy-start.3 = (bf16[128,16]{0,1:T(8,128)(2,1)S(1)}, bf16[128,16]{0,1:T(8,128)(2,1)}, u32[]{:S(2)}) copy-start(bf16[128,16]{0,1:T(8,128)(2,1)} %param.18) | copy-start | bytes 12292
  207.3 4.9 %copy-start.7 = (bf16[1,2048,256]{2,1,0:T(8,128)(2,1)S(1)}, bf16[1,2048,256]{2,1,0:T(8,128)(2,1)}, u32[]{:S(2)}) copy-start(bf16[1,2048,256]{2,1,0:T(8,128)(2,1)} %param.14) | copy-start | bytes 3145732
  208.1 13.1 %all-to-all-start.6 = ((bf16[4,128,512]{2,1,0:T(8,128)(2,1)}), bf16[4,128,512]{2,1,0:T(8,128)(2,1)S(1)}, u32[]{:S(2)}, u32[]{:S(2)}) async-start(bf16[4,128,512]{2,1,0:T(8,128)(2,1)} %bitcast.56), calls=%async_computation.6 | async-start | bytes 1048576 | tf_op jit(solution)/shard_map/all_to_all | solution.py:47
  212.1 2.8 copy-start.6
  212.2 2.8 copy-start.8
  221.3 1.2 copy-start.1
  222.5 20.2 %all-to-all-start.1 = ((bf16[4,640,256]{2,1,0:T(8,128)(2,1)}), bf16[4,640,256]{2,1,0:T(8,128)(2,1)S(1)}, u32[]{:S(2)}, u32[]{:S(2)}) async-start(bf16[4,640,256]{2,1,0:T(8,128)(2,1)} %broadcast_in_dim.56), calls=%async_computation.1 | async-start | bytes 2621440 | tf_op jit(solution)/shard_map/all_to_all | solution.py:17
  226.1 2.8 copy-start.5
  226.1 2.8 copy-start.9
  243.9 20.2 %all-to-all-start.4 = ((bf16[4,640,256]{2,1,0:T(8,128)(2,1)}), bf16[4,640,256]{2,1,0:T(8,128)(2,1)}, u32[]{:S(2)}, u32[]{:S(2)}) async-start(bf16[4,640,256]{2,1,0:T(8,128)(2,1)} %broadcast_in_dim.57), calls=%async_computation.4 | async-start | bytes 2621440 | tf_op jit(solution)/shard_map/all_to_all | solution.py:17
  264.1 41.2 %all-to-all-start.2 = ((bf16[128,5,512]{2,1,0:T(8,128)(2,1)}), bf16[128,5,512]{2,1,0:T(8,128)(2,1)S(1)}, u32[]{:S(2)}, u32[]{:S(2)}) async-start(bf16[128,5,512]{2,1,0:T(8,128)(2,1)} %copy.25), calls=%async_computation.2 | async-start | bytes 2097152 | tf_op jit(solution)/shard_map/all_to_all | solution.py:96
  281.8 29.9 %copy-start.4 = (f32[128,2]{0,1:T(2,128)S(1)}, f32[128,2]{0,1:T(2,128)}, u32[]{:S(2)}) copy-start(f32[128,2]{0,1:T(2,128)} %param.13) | copy-start | bytes 3076
  305.3 37.4 %all-to-all-start.5 = ((bf16[128,5,512]{2,1,0:T(8,128)(2,1)}), bf16[128,5,512]{2,1,0:T(8,128)(2,1)S(1)}, u32[]{:S(2)}, u32[]{:S(2)}) async-start(bf16[128,5,512]{2,1,0:T(8,128)(2,1)} %copy.28), calls=%async_computation.5 | async-start | bytes 2097152 | tf_op jit(solution)/shard_map/all_to_all | solution.py:96
Sparse Core Ops, SparseCore 0:
  70.0 33.7 all-gather.2
  108.6 37.8 all-gather.4
where the time goes:
time: 356 us; the launch traced here: 355 us
  blocking collectives  185 us (52%)
  waiting for transfers between devices  78.2 us (22%)
  local copies, waits for them, and re-layouts  29.1 us (8%)
  starting transfers between devices  28.6 us (8%)
  between operations  13.8 us (4%)
  matrix products  12.3 us (3%)
  other arithmetic  8.69 us (2%)
    all_to_all x2, blocking collectives, moved(): lax.all_to_all(group, axis, split_axis=split_dim, concat_axis=concat_dim,...  86.5 us
    all_to_all x2, waiting for transfers between devices, finish(): lax.all_to_all(partial_out.astype(jnp.bfloat16), 'ep', split_axis=0, conc...  51.8 us
    all_gather x1, blocking collectives, on_device(): whole_in = lax.all_gather(branch_in, 'ep', axis=0, tiled=True)  49.6 us
    all_gather x1, blocking collectives, on_device(): whole_out = lax.all_gather(branch_out, 'ep', axis=1, tiled=True)  48.7 us
    all_to_all x2, waiting for transfers between devices, copy_for_each(): lax.all_to_all(jnp.broadcast_to(x[None], (size, *x.shape)), axis, 0, 0, t...  20.9 us
    all_to_all x2, starting transfers between devices, finish(): lax.all_to_all(partial_out.astype(jnp.bfloat16), 'ep', split_axis=0, conc...  16.7 us
    all_to_all x2, starting transfers between devices, copy_for_each(): lax.all_to_all(jnp.broadcast_to(x[None], (size, *x.shape)), axis, 0, 0, t...  7.82 us
  transfers between devices with their start and end apart: 7, of which 5 were waited for; matrix products, arithmetic and copies ran while one was open for 8% of the time, Pallas kernels for 0%

commit v1 on v0

v1 whole, which is shorter than its diff:
```python
import functools

import jax
import jax.numpy as jnp
from jax import lax
from jax.experimental import pallas as pl
from jax.experimental.pallas import tpu as pltpu
from jax.sharding import PartitionSpec as P

NORM_EPSILON = 1e-06
GROUP = 4
CORES = 2
MESH_ID = pl.DeviceIdType.MESH


def round_up(n, m):
    return (n + m - 1) // m * m


def sigmoid(v):
    return 1.0 / (1.0 + jnp.exp(-v))


def floor_div(v, n):
    return jnp.floor((v + 0.5) * (1.0 / n))


def layer_kernel(
    zs_n,
    ys_n,
    xs_n,
    cap,
    tokens,
    gain,
    routes,
    routes_t,
    scores,
    bgate,
    bweights,
    w_gate,
    w_up,
    w_down,
    out,
    normed,
    zsend,
    zrecv,
    ysend,
    tok,
    w_gu,
    w_dn,
    hid,
    acc,
    psend,
    precv,
    half,
    qsend,
    qrecv,
    fsend,
    yback,
    zback,
    zgot,
    bw,
    bterm,
    bgot,
    local_sem,
    zd_s,
    zd_r,
    yd_s,
    yd_r,
    tx_s,
    tx_r,
    tc_s,
    tc_r,
    hx_s,
    hx_r,
    pc_s,
    pc_r,
    qy_s,
    qy_r,
    fy_s,
    fy_r,
    zb_s,
    zb_r,
    by_s,
    by_r,
    bz_s,
    bz_r,
    bc_s,
    bc_r,
    bx_s,
    bx_r,
):
    f32, bf16 = jnp.float32, jnp.bfloat16
    ep = lax.axis_index("ep")
    x = lax.axis_index("tp")
    c = lax.rem(ep, CORES)
    y = lax.rem(ep // CORES, ys_n)
    z = ep // (CORES * ys_n)
    pairs = ys_n // 2
    pair = y // 2
    h = lax.rem(y, 2)
    rows_tok, width = tokens.shape
    dx = width // xs_n
    fx = w_gate.shape[2]
    experts = zs_n * pairs
    zrow = zsend.shape[1]
    erow = ysend.shape[1]

    def at(z_, y_, c_, x_):
        return ((z_ * ys_n + y_) * CORES + c_, x_)

    def zpeer(r):
        return lax.rem(z + r, zs_n)

    def ypeer(r):
        return lax.rem(y + r, ys_n)

    def xpeer(r):
        return lax.rem(x + r, xs_n)

    def remote(src, dst, s, r, dev):
        return pltpu.make_async_remote_copy(
            src_ref=src, dst_ref=dst, send_sem=s, recv_sem=r, device_id=dev, device_id_type=MESH_ID
        )

    barrier = pltpu.get_barrier_semaphore()
    peers = [at(zpeer(r), y, c, x) for r in range(1, zs_n)]
    peers += [at(z, ypeer(r), c, x) for r in range(1, ys_n)]
    peers += [at(z, y, c, xpeer(r)) for r in range(1, xs_n)]
    peers += [at(z, y, 1 - c, x)]
    for dev in peers:
        pl.semaphore_signal(barrier, inc=1, device_id=dev, device_id_type=MESH_ID)

    weights = [
        pltpu.make_async_copy(w_gate.at[0], w_gu.at[:, pl.ds(0, fx)], local_sem.at[0]),
        pltpu.make_async_copy(w_up.at[0], w_gu.at[:, pl.ds(fx, fx)], local_sem.at[1]),
        pltpu.make_async_copy(w_down.at[0], w_dn, local_sem.at[2]),
    ]
    for copy in weights:
        copy.start()

    tf = tokens[...].astype(f32)
    scaled = lax.rsqrt(jnp.sum(tf * tf, axis=-1, keepdims=True) * (1.0 / width) + NORM_EPSILON)
    nf = (tf * scaled * gain[...]).astype(bf16)
    normed[...] = nf
    bsum = jnp.sum(nf.astype(f32) * bgate[...], axis=-1, keepdims=True)
    branch_weight = sigmoid(bsum)

    def positions(r0, r1, axis):
        shape = (experts, rows_tok) if axis == 0 else (rows_tok, experts)
        ids = lax.broadcasted_iota(jnp.int32, shape, axis)
        c0 = jnp.where(ids == r0, 1.0, 0.0)
        c1 = jnp.where(ids == r1, 1.0, 0.0)
        sq = (rows_tok, rows_tok)
        a = lax.broadcasted_iota(jnp.int32, sq, 0)
        b = lax.broadcasted_iota(jnp.int32, sq, 1)
        both = (c0 + c1).astype(bf16)
        if axis == 0:
            earlier = jnp.where(a < b, 1.0, 0.0).astype(bf16)
            rank = jnp.dot(both, earlier, preferred_element_type=f32)
        else:
            earlier = jnp.where(b < a, 1.0, 0.0).astype(bf16)
            rank = jnp.dot(earlier, both, preferred_element_type=f32)

        def place(ch, r):
            e = r.astype(f32)
            zz = floor_div(e, pairs)
            base = zz * zrow + (e - zz * pairs) * cap
            return jnp.sum(ch * rank, axis=axis, keepdims=True) + base

        return place(c0, r0), place(c1, r1)

    p0, p1 = positions(routes_t[0:1, :], routes_t[1:2, :], 0)
    slots = zs_n * zrow
    srow = lax.broadcasted_iota(jnp.int32, (slots, rows_tok), 0).astype(f32)
    pick = jnp.where((srow == p0) | (srow == p1), 1.0, 0.0).astype(bf16)
    own_cols = pl.ds(pl.multiple_of(x * dx, dx), dx)
    packed = jnp.dot(pick, normed[:, own_cols], preferred_element_type=f32).astype(bf16)
    zsend[...] = packed.reshape(zs_n, zrow, dx)

    pl.semaphore_wait(barrier, len(peers))

    zd = []
    for r in range(1, zs_n):
        zt = zpeer(r)
        copy = remote(
            zsend.at[zt], zrecv.at[z], zd_s.at[r], zd_r.at[r], at(zt, y, c, x)
        )
        copy.start()
        zd.append(copy)
    by = []
    for r in range(1, ys_n):
        copy = remote(
            bweights, bw.at[:, z, y, c], by_s.at[r], by_r.at[r], at(z, ypeer(r), c, x)
        )
        copy.start()
        by.append(copy)
    bw[:, z, y, c] = bweights[...]
    zrecv[z] = zsend[z]

    def row_target(q):
        pp = floor_div(q, erow)
        rem = q - pp * erow
        zz = floor_div(rem, cap)
        return jnp.where(zz < zs_n, zz * zrow + pp * cap + (rem - zz * cap), -1.0)

    qcol = lax.broadcasted_iota(jnp.int32, (pairs * erow, slots), 0).astype(f32)
    qlane = lax.broadcasted_iota(jnp.int32, (pairs * erow, slots), 1).astype(f32)
    repack = jnp.where(row_target(qcol) == qlane, 1.0, 0.0).astype(bf16)

    for copy in zd:
        copy.wait_recv()
    arrived = zrecv[...].reshape(slots, dx)
    moved = jnp.dot(repack, arrived, preferred_element_type=f32).astype(bf16)
    ysend[...] = moved.reshape(pairs, erow, dx)

    yd = []
    for r in range(1, ys_n):
        yt = ypeer(r)
        pt = yt // 2
        d = lax.rem(y + ys_n - 2 * pt, ys_n)
        k = jnp.where(d <= pairs, jnp.maximum(2 * d - 1, 0), 2 * (ys_n - d))
        copy = remote(
            ysend.at[pt],
            tok.at[k, c, :, own_cols],
            yd_s.at[r],
            yd_r.at[k],
            at(z, yt, c, x),
        )
        copy.start()
        yd.append(copy)
    tok[h, c, :, own_cols] = ysend[pair]

    for copy in by:
        copy.wait_recv()
    bz = []
    for r in range(1, zs_n):
        zt = zpeer(r)
        part = bw.at[:, z, :, c]
        copy = remote(part, part, bz_s.at[r], bz_r.at[r], at(zt, y, c, x))
        copy.start()
        bz.append(copy)

    east, west = at(z, y, c, xpeer(1)), at(z, y, c, xpeer(xs_n - 1))
    partner = at(z, y, 1 - c, x)
    started = []

    def tok_part(k, xx):
        return tok.at[k, c, :, pl.ds(pl.multiple_of(xx * dx, dx), dx)]

    def hid_part(k, xx):
        return hid.at[k, :, :, pl.ds(pl.multiple_of(xx * fx, fx), fx)]

    def spread(part, sems, rsems, k):
        for way, dev in ((0, east), (1, west)):
            copy = remote(part(k, x), part(k, x), sems.at[way, k], rsems.at[way, k], dev)
            copy.start()
            started.append(copy)

    def arrive(part, rsems, sems, way, k):
        ref = part(k, x)
        remote(ref, ref, sems.at[way, k], rsems.at[way, k], east).wait_recv()

    def relay(part, sems, rsems, k):
        way = k % 2
        arrive(part, rsems, sems, way, k)
        ref = part(k, xpeer(xs_n - 1) if way == 0 else xpeer(1))
        copy = remote(
            ref, ref, sems.at[2, k], rsems.at[2, k], east if way == 0 else west
        )
        copy.start()
        started.append(copy)

    def settle(part, sems, rsems, k):
        arrive(part, rsems, sems, 1 - k % 2, k)
        arrive(part, rsems, sems, 2, k)

    def step_a(k):
        if k == 1:
            kk = 1 - h
            for step in (0, 1):
                if step == 1:
                    ref = tok.at[kk, c, :, own_cols]
                    remote(ref, ref, yd_s.at[0], yd_r.at[kk], partner).wait_recv()
                    which = kk
                else:
                    which = h
                ref = tok.at[which, c, :, own_cols]
                for way, dev in ((0, east), (1, west)):
                    copy = remote(ref, ref, tx_s.at[way, which], tx_r.at[way, which], dev)
                    copy.start()
                    started.append(copy)
        elif k > 1:
            ref = tok.at[k, c, :, own_cols]
            remote(ref, ref, yd_s.at[0], yd_r.at[k], partner).wait_recv()
            spread(tok_part, tx_s, tx_r, k)

    def step_b(k):
        relay(tok_part, tx_s, tx_r, k)

    def step_c(k):
        settle(tok_part, tx_s, tx_r, k)
        ref = tok.at[k, c]
        copy = remote(ref, ref, tc_s.at[k], tc_r.at[k], partner)
        copy.start()
        started.append(copy)

    def step_e(j):
        for k in (2 * j, 2 * j + 1):
            ref = tok.at[k, 1 - c]
            remote(ref, ref, tc_s.at[k], tc_r.at[k], partner).wait_recv()
        if j == 0:
            weights[0].wait()
            weights[1].wait()
        rows = tok[2 * j : 2 * j + 2].reshape(2 * CORES * erow, width)
        pre = jnp.dot(rows, w_gu[...], preferred_element_type=f32)
        gate, up = pre[:, :fx], pre[:, fx:]
        hidden = (gate / (1.0 + jnp.exp(-gate)) * up).astype(bf16)
        cols = pl.ds(pl.multiple_of(x * fx, fx), fx)
        hid[2 * j : 2 * j + 2, :, :, cols] = hidden.reshape(2, CORES, erow, fx)
        for k in (2 * j, 2 * j + 1):
            spread(hid_part, hx_s, hx_r, k)

    def step_f(k):
        relay(hid_part, hx_s, hx_r, k)

    def step_g(j):
        for k in (2 * j, 2 * j + 1):
            settle(hid_part, hx_s, hx_r, k)
        if j == 0:
            weights[2].wait()
        rows = hid[2 * j : 2 * j + 2].reshape(2 * CORES * erow, hid.shape[3])
        part = jnp.dot(rows, w_dn[...], preferred_element_type=f32)
        part = part.reshape(2, CORES, erow, dx)
        acc[...] = part
        psend[2 * j : 2 * j + 2] = part.astype(bf16)
        copy = remote(
            psend.at[pl.ds(2 * j, 2), 1 - c],
            precv.at[pl.ds(2 * j, 2)],
            pc_s.at[j],
            pc_r.at[j],
            partner,
        )
        copy.start()
        started.append(copy)
        return copy

    def step_i(j, copy):
        copy.wait_recv()
        total = acc[:, c] + precv[2 * j : 2 * j + 2].astype(f32)
        half[j] = total
        qsend[2 * j : 2 * j + 2] = total.astype(bf16)
        other = at(z, y + 1 - 2 * h, c, x)
        copy = remote(
            qsend.at[2 * j + 1 - h], qrecv.at[j], qy_s.at[j], qy_r.at[j], other
        )
        copy.start()
        started.append(copy)
        return copy

    def step_j(j, copy):
        copy.wait_recv()
        done = (half[j, h] + qrecv[j].astype(f32)).astype(bf16)
        if j == 0:
            yback[pair] = done
            return
        fsend[j] = done
        back = lax.rem(y + ys_n + j * (2 * h - 1), ys_n)
        copy = remote(fsend.at[j], yback.at[pair], fy_s.at[j], fy_r.at[j], at(z, back, c, x))
        copy.start()
        started.append(copy)
        backs.append(copy)

    backs = []
    nj = pairs
    pend_g, pend_i = {}, {}

    def branch_core():
        for copy in bz:
            copy.wait_recv()
        copy = remote(bw.at[:, :, :, c], bw.at[:, :, :, c], bc_s.at[0], bc_r.at[0], partner)
        copy.start()
        started.append(copy)

    def branch_dense():
        ref = bw.at[:, :, :, 1 - c]
        remote(ref, ref, bc_s.at[0], bc_r.at[0], partner).wait_recv()
        whole_in = bw[0].reshape(width, bw.shape[5])
        pre = jnp.dot(normed[...], whole_in, preferred_element_type=f32)
        hb = (pre / (1.0 + jnp.exp(-pre))).astype(bf16)
        for xx in range(xs_n):
            zpart = zs_n // xs_n if zs_n >= xs_n else 0
            if zpart:
                wo = bw[1, xx * zpart : (xx + 1) * zpart].reshape(dx, bw.shape[5])
            else:
                wo = bw[1].reshape(width, bw.shape[5])[xx * dx : (xx + 1) * dx]
            term = lax.dot_general(hb, wo, (((1,), (1,)), ((), ())), preferred_element_type=f32)
            bterm[xx] = term.astype(bf16)

    bx = []

    def branch_send():
        for r in range(1, xs_n):
            xt = xpeer(r)
            copy = remote(bterm.at[xt], bgot.at[r], bx_s.at[r], bx_r.at[r], at(z, y, c, xt))
            copy.start()
            bx.append(copy)

    for k in (0, 1):
        step_a(k)
    for j in range(nj):
        nxt = (2 * j + 2, 2 * j + 3)
        for k in (2 * j, 2 * j + 1):
            step_b(k)
        if j + 1 < nj:
            for k in nxt:
                step_a(k)
        for k in (2 * j, 2 * j + 1):
            step_c(k)
        if j == min(1, nj - 1):
            branch_core()
        step_e(j)
        if j > 0:
            for k in (2 * j - 2, 2 * j - 1):
                step_f(k)
    branch_dense()
    last = nj - 1
    for k in (2 * last, 2 * last + 1):
        step_f(k)
    branch_send()
    for j in range(nj):
        pend = step_g(j)
        pend = step_i(j, pend)
        step_j(j, pend)

    tlane = lax.broadcasted_iota(jnp.int32, (slots, pairs * erow), 0).astype(f32)
    trow = lax.broadcasted_iota(jnp.int32, (slots, pairs * erow), 1).astype(f32)
    unpack = jnp.where(row_target(trow) == tlane, 1.0, 0.0).astype(bf16)
    for copy in backs:
        copy.wait_recv()
    back_rows = yback[...].reshape(pairs * erow, dx)
    zout = jnp.dot(unpack, back_rows, preferred_element_type=f32).astype(bf16)
    zback[...] = zout.reshape(zs_n, zrow, dx)
    zb = []
    for r in range(1, zs_n):
        zt = zpeer(r)
        copy = remote(zback.at[zt], zgot.at[z], zb_s.at[r], zb_r.at[r], at(zt, y, c, x))
        copy.start()
        zb.append(copy)
    zgot[z] = zback[z]

    for copy in bx:
        copy.wait_recv()
    share = bterm[x].astype(f32)
    for r in range(1, xs_n):
        share = share + bgot[r].astype(f32)
    share = share * branch_weight
    q0, q1 = positions(routes[:, 0:1], routes[:, 1:2], 1)
    slane = lax.broadcasted_iota(jnp.int32, (rows_tok, slots), 1).astype(f32)
    g0 = jnp.where(slane == q0, 1.0, 0.0).astype(bf16)
    g1 = jnp.where(slane == q1, 1.0, 0.0).astype(bf16)
    diff = scores[:, 0:1] - scores[:, 1:2]
    w0, w1 = sigmoid(diff), sigmoid(-diff)
    for copy in zb:
        copy.wait_recv()
    got = zgot[...].reshape(slots, dx)
    r0 = jnp.dot(g0, got, preferred_element_type=f32)
    r1 = jnp.dot(g1, got, preferred_element_type=f32)
    out[...] = (w0 * r0 + w1 * r1 + share).astype(out.dtype)

    for copy in zd + by + yd + bz + started + bx + zb:
        copy.wait_send()


def on_device(
    cores_z,
    cores_y,
    tokens,
    norm_gain,
    routes,
    route_scores,
    expert_gate,
    expert_up,
    expert_down,
    branch_in,
    branch_out,
    branch_gate,
):
    zs_n, ys_n = cores_z, cores_y
    xs_n = lax.axis_size("tp")
    rows_tok, width = tokens.shape
    experts = zs_n * ys_n // 2
    cap = 5 * rows_tok * routes.shape[1] // (4 * experts)
    pairs = ys_n // 2
    dx = width // xs_n
    fx = expert_gate.shape[2]
    fg = expert_down.shape[1]
    zrow = round_up(pairs * cap, 16)
    erow = round_up(zs_n * cap, 16)
    brow = branch_in.shape[0]
    bcol = branch_in.shape[1]
    bweights = jnp.stack([branch_in, branch_out.T])
    bf16, f32 = jnp.bfloat16, jnp.float32
    vm = lambda shape, dtype=bf16: pltpu.VMEM(shape, dtype)
    sem = lambda *shape: pltpu.SemaphoreType.DMA(shape)
    scratch = [
        vm((rows_tok, width)),
        vm((zs_n, zrow, dx)),
        vm((zs_n, zrow, dx)),
        vm((pairs, erow, dx)),
        vm((ys_n, CORES, erow, width)),
        vm((width, 2 * fx)),
        vm((fg, dx)),
        vm((ys_n, CORES, erow, fg)),
        vm((2, CORES, erow, dx), f32),
        vm((ys_n, CORES, erow, dx)),
        vm((ys_n, erow, dx)),
        vm((pairs, 2, erow, dx), f32),
        vm((ys_n, erow, dx)),
        vm((pairs, erow, dx)),
        vm((pairs, erow, dx)),
        vm((pairs, erow, dx)),
        vm((zs_n, zrow, dx)),
        vm((zs_n, zrow, dx)),
        vm((2, zs_n, ys_n, CORES, brow, bcol)),
        vm((xs_n, rows_tok, dx)),
        vm((xs_n, rows_tok, dx)),
        sem(3),
        sem(zs_n),
        sem(zs_n),
        sem(ys_n),
        sem(ys_n),
        sem(3, ys_n),
        sem(3, ys_n),
        sem(ys_n),
        sem(ys_n),
        sem(3, ys_n),
        sem(3, ys_n),
        sem(pairs),
        sem(pairs),
        sem(pairs),
        sem(pairs),
        sem(pairs),
        sem(pairs),
        sem(zs_n),
        sem(zs_n),
        sem(ys_n),
        sem(ys_n),
        sem(zs_n),
        sem(zs_n),
        sem(1),
        sem(1),
        sem(xs_n),
        sem(xs_n),
    ]
    in_vmem = pl.BlockSpec(memory_space=pltpu.VMEM)
    in_hbm = pl.BlockSpec(memory_space=pl.ANY)
    return pl.pallas_call(
        functools.partial(layer_kernel, zs_n, ys_n, xs_n, cap),
        out_shape=jax.ShapeDtypeStruct((rows_tok, dx), bf16),
        in_specs=[in_vmem] * 7 + [in_hbm] * 3,
        out_specs=in_vmem,
        scratch_shapes=scratch,
        compiler_params=pltpu.CompilerParams(
            collective_id=0, has_side_effects=True, vmem_limit_bytes=60 * 1024 * 1024
        ),
        name="routed_layer",
    )(
        tokens,
        norm_gain.reshape(1, -1),
        routes,
        routes.T,
        route_scores,
        branch_gate.reshape(1, -1),
        bweights,
        expert_gate,
        expert_up,
        expert_down,
    )


def solution(mesh, z_y=None):
    ep = mesh.shape["ep"]
    zs_n, ys_n = z_y or (8, ep // (8 * CORES))
    in_specs = (
        P("ep", None),
        P(),
        P("ep", None),
        P("ep", None),
        P("ep", None, "tp"),
        P("ep", None, "tp"),
        P("ep", None, "tp"),
        P("ep", "tp"),
        P("tp", "ep"),
        P(),
    )
    return jax.shard_map(
        functools.partial(on_device, zs_n, ys_n),
        mesh=mesh,
        in_specs=in_specs,
        out_specs=P("ep", "tp"),
        check_vma=False,
    )
```

time: 356 us -> 134 us (0.38)
  blocking collectives: 185 us -> 0 us
  Pallas kernels: 0 us -> 127 us
  waiting for transfers between devices: 78.2 us -> 0 us
  starting transfers between devices: 28.6 us -> 0 us
  local copies, waits for them, and re-layouts: 29.1 us -> 3.83 us
  between operations: 13.8 us -> 0.01 us
  matrix products: 12.3 us -> 0 us
  other arithmetic: 8.69 us -> 0.59 us
    pallas_call x0 -> x1, Pallas kernels: none -> 127 us  [on_device(): pl.pallas_call(functools.partial(layer_kernel, zs_n, ys_n, xs_n, cap), ou...]
    all_gather x2 -> x0, blocking collectives: 98.2 us -> none  [the longest x1 49.6 us: on_device(): whole_in = lax.all_gather(branch_in, 'ep', axis=0, tiled=True)]
    all_to_all x2 -> x0, blocking collectives: 86.5 us -> none  [moved(): lax.all_to_all(group, axis, split_axis=split_dim, concat_axis=concat_dim,...]
    all_to_all x5 -> x0, waiting for transfers between devices: 78.1 us -> none  [the longest x2 51.8 us: finish(): lax.all_to_all(partial_out.astype(jnp.bfloat16), 'ep', split_axis=0, conc...]
    all_to_all x5 -> x0, starting transfers between devices: 28.5 us -> none  [the longest x2 16.7 us: finish(): lax.all_to_all(partial_out.astype(jnp.bfloat16), 'ep', split_axis=0, conc...]
    dot_general x7 -> x0, matrix products: 12.3 us -> none  [the longest x2 5.47 us: expert_columns(): jnp.dot(part_rows, w_gate, preferred_element_type=jnp.float32)]
    reduce_sum x6 -> x0, other arithmetic: 6.43 us -> none  [the longest x1 1.85 us: on_device(): jnp.sum(returned.reshape(expert_count, group_size, capacity, -1), axis=1)]
    dot_general x2 -> x0, local copies, waits for them, and re-layouts: 4.95 us -> none  [finish(): jnp.dot(collect(hidden, 'tp', 1), w_down, preferred_element_type=jnp.floa...]
  transfers between devices with their start and end apart: 7 -> 0, of which waited for: 5 -> 0; matrix products, arithmetic and copies ran while one was open for 8% -> 0% of each run, Pallas kernels for 0% -> 0%
where the time goes in v1:
time: 134 us; the launch traced here: 132 us
  Pallas kernels  127 us (95%)
  local copies, waits for them, and re-layouts  3.83 us (3%)
    pallas_call x1, Pallas kernels, on_device(): pl.pallas_call(functools.partial(layer_kernel, zs_n, ys_n, xs_n, cap), ou...  127 us
    unnamed x11, local copies, waits for them, and re-layouts  3.83 us

profile of v1, /device:TPU:1, one launch (start us, length us, event | category | flops | bytes accessed | tf_op | source)
XLA Modules:
  0.0 131.7 jit_solution(12905375083217790579)
XLA Ops:
  0.0 0.0 copy-start.2
  0.0 0.0 copy-start.1
  0.0 0.7 copy-done.2
  0.7 0.0 copy-done.1
  0.7 0.0 copy-start.3
  0.7 0.6 pad_maximum_fusion.bweights
  1.3 0.1 copy-done.3
  1.4 0.0 copy-start
  1.4 0.7 copy.12.scores
  2.1 0.0 copy-done
  2.1 0.7 copy.11.routes
  2.9 127.2 %routed_layer.1 = bf16[128,512]{1,0:T(8,128)(2,1)} custom-call(bf16[128,2048]{1,0:T(8,128)(2,1)} %tokens.1, f32[1,2048]{1,0:T(1,128)} %bitcast.7, s32[128,2]{1,0:T(8,128)} %copy.11.routes, s32[2,128]{1,0:T(2,128)} %bitcast.9, f32[128,2]{1,0:T(8,128)} %copy.12.scores, f32[1,2048]{1,0:T(1,128)} %bitcast.8, bf16[2,16,128]{2,1,0:T(8,128)(2,1)} %pad_maximum_fusion.bweights, ...), custom_call_target="tpu_custom_call" | custom-call | tf_op jit(solution)/shard_map/routed_layer/pallas_call | solution.py:558
  130.1 1.6 %copy.14 = bf16[128,512]{1,0:T(8,128)(2,1)} copy(bf16[128,512]{1,0:T(8,128)(2,1)} %routed_layer.1) | data formatting | bytes 262144
Async XLA Ops:
  0.0 0.7 copy-start.2
  0.0 0.7 copy-start.1
  0.7 0.7 copy-start.3
  1.4 0.7 copy-start

commit v2 on v1

v2 whole, which is shorter than its diff:
```python
import functools

import jax
import jax.numpy as jnp
from jax import lax
from jax.experimental import pallas as pl
from jax.experimental.pallas import tpu as pltpu
from jax.sharding import PartitionSpec as P

NORM_EPSILON = 1e-06
GROUP = 4
CORES = 2
MESH_ID = pl.DeviceIdType.MESH


def round_up(n, m):
    return (n + m - 1) // m * m


def sigmoid(v):
    return 1.0 / (1.0 + jnp.exp(-v))


def floor_div(v, n):
    return jnp.floor((v + 0.5) * (1.0 / n))


def layer_kernel(
    zs_n,
    ys_n,
    xs_n,
    cap,
    tokens,
    gain,
    routes_t,
    scores_t,
    bgate,
    b_in,
    b_out,
    w_gate,
    w_up,
    w_down,
    out,
    normed,
    zsend_a,
    zsend_b,
    zrecv_a,
    zrecv_b,
    ysend,
    tok,
    w_gu,
    w_dn,
    hid,
    acc,
    psend,
    precv,
    half,
    qsend,
    qrecv,
    fsend,
    yback,
    zback_a,
    zback_b,
    zgot_a,
    zgot_b,
    bw,
    bterm,
    bgot,
    local_sem,
    za_s,
    za_r,
    zd_s,
    zd_r,
    yd_s,
    yd_r,
    tx_s,
    tx_r,
    tc_s,
    tc_r,
    hx_s,
    hx_r,
    pc_s,
    pc_r,
    qy_s,
    qy_r,
    fy_s,
    fy_r,
    zb_s,
    zb_r,
    zc_s,
    zc_r,
    by_s,
    by_r,
    bz_s,
    bz_r,
    bc_s,
    bc_r,
    bx_s,
    bx_r,
):
    f32, bf16 = jnp.float32, jnp.bfloat16
    ep = lax.axis_index("ep")
    x = lax.axis_index("tp")
    c = lax.rem(ep, CORES)
    y = lax.rem(ep // CORES, ys_n)
    z = ep // (CORES * ys_n)
    pairs = ys_n // 2
    pair = y // 2
    h = lax.rem(y, 2)
    hops = [0] + list(range(2, pairs)) + [1]
    rows_tok, width = tokens.shape
    dx = width // xs_n
    fx = w_gate.shape[2]
    experts = zs_n * pairs
    arow = zsend_a.shape[1]
    brow = zsend_b.shape[1]
    a_slots, b_slots = zs_n * arow, zs_n * brow
    erow = ysend.shape[1]
    mates = pairs - 1

    def at(z_, y_, c_, x_):
        return ((z_ * ys_n + y_) * CORES + c_, x_)

    def zpeer(r):
        return lax.rem(z + r, zs_n)

    def ypeer(r):
        return lax.rem(y + r, ys_n)

    def xpeer(r):
        return lax.rem(x + r, xs_n)

    def remote(src, dst, s, r, dev):
        return pltpu.make_async_remote_copy(
            src_ref=src, dst_ref=dst, send_sem=s, recv_sem=r, device_id=dev, device_id_type=MESH_ID
        )

    barrier = pltpu.get_barrier_semaphore()
    peers = [at(zpeer(r), y, c, x) for r in range(1, zs_n)]
    peers += [at(z, ypeer(r), c, x) for r in range(1, ys_n)]
    peers += [at(z, y, c, xpeer(r)) for r in range(1, xs_n)]
    peers += [at(z, y, 1 - c, x)]
    for dev in peers:
        pl.semaphore_signal(barrier, inc=1, device_id=dev, device_id_type=MESH_ID)

    weights = [
        pltpu.make_async_copy(w_gate.at[0], w_gu.at[:, pl.ds(0, fx)], local_sem.at[0]),
        pltpu.make_async_copy(w_up.at[0], w_gu.at[:, pl.ds(fx, fx)], local_sem.at[1]),
        pltpu.make_async_copy(w_down.at[0], w_dn, local_sem.at[2]),
    ]
    for copy in weights:
        copy.start()

    tf = tokens[...].astype(f32)
    scaled = lax.rsqrt(jnp.sum(tf * tf, axis=-1, keepdims=True) * (1.0 / width) + NORM_EPSILON)
    nf = (tf * scaled * gain[...]).astype(bf16)
    normed[...] = nf

    ids = lax.broadcasted_iota(jnp.int32, (experts, rows_tok), 0)
    sq = (rows_tok, rows_tok)
    sq_a = lax.broadcasted_iota(jnp.int32, sq, 0)
    sq_b = lax.broadcasted_iota(jnp.int32, sq, 1)
    chosen = [jnp.where(ids == routes_t[r : r + 1, :], 1.0, 0.0) for r in (0, 1)]
    earlier = jnp.where(sq_a < sq_b, 1.0, 0.0).astype(bf16)
    ranks = jnp.dot((chosen[0] + chosen[1]).astype(bf16), earlier, preferred_element_type=f32)
    go, come = [], []
    for r in (0, 1):
        rank = jnp.sum(chosen[r] * ranks, axis=0, keepdims=True)
        e = routes_t[r : r + 1, :].astype(f32)
        zz = floor_div(e, pairs)
        v = (e - zz * pairs - pair.astype(f32)) * (1 - 2 * h).astype(f32) + pairs
        rel = jnp.where(v >= pairs, v - pairs, v)
        go.append(
            rank
            + jnp.where(rel < 0.5, zz * arow, a_slots + zz * brow + (rel - 1.0) * cap)
        )
        come.append(
            rank
            + jnp.where(rel < mates - 0.5, zz * brow + rel * cap, b_slots + zz * arow)
        )
    srow = lax.broadcasted_iota(jnp.int32, (a_slots + b_slots, rows_tok), 0).astype(f32)
    pick = jnp.where((srow == go[0]) | (srow == go[1]), 1.0, 0.0).astype(bf16)
    own_cols = pl.ds(pl.multiple_of(x * dx, dx), dx)
    packed = jnp.dot(pick, normed[:, own_cols], preferred_element_type=f32).astype(bf16)
    zsend_a[...] = packed[:a_slots].reshape(zs_n, arow, dx)
    zsend_b[...] = packed[a_slots:].reshape(zs_n, brow, dx)

    pl.semaphore_wait(barrier, len(peers))

    za, zd, by = [], [], []
    near = sorted(range(1, zs_n), key=lambda r: min(r, zs_n - r))
    for src, dst, ss, rs, kept in (
        (zsend_a, zrecv_a, za_s, za_r, za),
        (zsend_b, zrecv_b, zd_s, zd_r, zd),
    ):
        for copy in za:
            copy.wait_send()
        for r in near:
            zt = zpeer(r)
            copy = remote(src.at[zt], dst.at[z], ss.at[r], rs.at[r], at(zt, y, c, x))
            copy.start()
            kept.append(copy)
    for r in range(1, ys_n):
        for w, part in enumerate((b_in, b_out)):
            copy = remote(
                part, bw.at[w, z, y, c], by_s.at[w, r], by_r.at[w, r], at(z, ypeer(r), c, x)
            )
            copy.start()
            by.append(copy)
    bw[0, z, y, c] = b_in[...]
    bw[1, z, y, c] = b_out[...]
    zrecv_a[z] = zsend_a[z]
    zrecv_b[z] = zsend_b[z]

    bsum = jnp.sum(normed[...].astype(f32) * bgate[...], axis=-1, keepdims=True)
    branch_weight = sigmoid(bsum)

    def row_target(q, step):
        pp = floor_div(q, erow)
        rem = q - pp * erow
        zz = floor_div(rem, cap)
        return jnp.where(zz < zs_n, zz * step + pp * cap + (rem - zz * cap), -1.0)

    def permutation(rows, slots, step):
        q = lax.broadcasted_iota(jnp.int32, (rows, slots), 0).astype(f32)
        t = lax.broadcasted_iota(jnp.int32, (rows, slots), 1).astype(f32)
        return jnp.where(row_target(q, step) == t, 1.0, 0.0).astype(bf16)

    def unpermutation(rows, slots, step):
        q = lax.broadcasted_iota(jnp.int32, (slots, rows), 1).astype(f32)
        t = lax.broadcasted_iota(jnp.int32, (slots, rows), 0).astype(f32)
        return jnp.where(row_target(q, step) == t, 1.0, 0.0).astype(bf16)

    east, west = at(z, y, c, xpeer(1)), at(z, y, c, xpeer(xs_n - 1))
    partner = at(z, y, 1 - c, x)
    mate = at(z, y + 1 - 2 * h, c, x)
    started, backs, bz, bx, backs_z = [], [], [], [], []
    pending = {}

    def begin(copy):
        copy.start()
        started.append(copy)
        return copy

    def tok_part(k, xx):
        return tok.at[k, c, :, pl.ds(pl.multiple_of(xx * dx, dx), dx)]

    def hid_part(k, xx):
        return hid.at[k, :, :, pl.ds(pl.multiple_of(xx * fx, fx), fx)]

    def spread(part, sems, rsems, k):
        for way, dev in ((0, east), (1, west)):
            begin(remote(part(k, x), part(k, x), sems.at[way, k], rsems.at[way, k], dev))

    def arrive(part, rsems, sems, way, k):
        ref = part(k, x)
        remote(ref, ref, sems.at[way, k], rsems.at[way, k], east).wait_recv()

    def relay(part, sems, rsems, k):
        way = k % 2
        arrive(part, rsems, sems, way, k)
        ref = part(k, xpeer(xs_n - 1) if way == 0 else xpeer(1))
        begin(remote(ref, ref, sems.at[2, k], rsems.at[2, k], east if way == 0 else west))

    def settle(part, sems, rsems, k):
        arrive(part, rsems, sems, 1 - k % 2, k)
        arrive(part, rsems, sems, 2, k)

    def y_wait(k):
        ref = tok.at[k, c, :, own_cols]
        remote(ref, ref, yd_s.at[0], yd_r.at[k], mate).wait_recv()

    def both(i):
        return (2 * i, 2 * i + 1)

    def own_pair():
        with jax.named_scope("za_wait"):
            for copy in za:
                copy.wait_recv()
        first = permutation(erow, a_slots, arow)
        moved = jnp.dot(first, zrecv_a[...].reshape(a_slots, dx), preferred_element_type=f32)
        tok[h, c, :, own_cols] = moved.astype(bf16)
        ref = tok.at[h, c, :, own_cols]
        begin(remote(ref, ref, yd_s.at[0], yd_r.at[h], mate))
        spread(tok_part, tx_s, tx_r, h)
        with jax.named_scope("y_wait_mate"):
            y_wait(1 - h)
        spread(tok_part, tx_s, tx_r, 1 - h)

    def other_pairs():
        rest = permutation(mates * erow, b_slots, brow)
        with jax.named_scope("zb_wait"):
            for copy in zd:
                copy.wait_recv()
        moved = jnp.dot(rest, zrecv_b[...].reshape(b_slots, dx), preferred_element_type=f32)
        ysend[...] = moved.astype(bf16).reshape(mates, erow, dx)
        for i in range(1, pairs):
            pt = lax.rem(pair + pairs + i * (1 - 2 * h), pairs)
            k = 2 * i + lax.rem(h + hops[i], 2)
            for hh in (0, 1):
                begin(
                    remote(
                        ysend.at[i - 1],
                        tok.at[k, c, :, own_cols],
                        yd_s.at[2 * i + hh],
                        yd_r.at[k],
                        at(z, 2 * pt + hh, c, x),
                    )
                )

    def branch_planes():
        for copy in by:
            copy.wait_recv()
        for r in range(1, zs_n):
            part = bw.at[:, z, :, c]
            copy = remote(part, part, bz_s.at[r], bz_r.at[r], at(zpeer(r), y, c, x))
            copy.start()
            bz.append(copy)

    def step_a(i):
        for k in both(i):
            with jax.named_scope(f"a_wait{k}"):
                y_wait(k)
            spread(tok_part, tx_s, tx_r, k)

    def step_b(i):
        for k in both(i):
            with jax.named_scope(f"b_relay{k}"):
                relay(tok_part, tx_s, tx_r, k)

    def step_c(i):
        for k in both(i):
            with jax.named_scope(f"c_settle{k}"):
                settle(tok_part, tx_s, tx_r, k)
            ref = tok.at[k, c]
            begin(remote(ref, ref, tc_s.at[k], tc_r.at[k], partner))

    def step_e(i):
        with jax.named_scope(f"e_wait{i}"):
            for k in both(i):
                ref = tok.at[k, 1 - c]
                remote(ref, ref, tc_s.at[k], tc_r.at[k], partner).wait_recv()
            if i == 0:
                weights[0].wait()
                weights[1].wait()
        with jax.named_scope(f"e_dot{i}"):
            rows = tok[2 * i : 2 * i + 2].reshape(2 * CORES * erow, width)
            pre = jnp.dot(rows, w_gu[...], preferred_element_type=f32)
            gate, up = pre[:, :fx], pre[:, fx:]
            hidden = (gate / (1.0 + jnp.exp(-gate)) * up).astype(bf16)
            cols = pl.ds(pl.multiple_of(x * fx, fx), fx)
            hid[2 * i : 2 * i + 2, :, :, cols] = hidden.reshape(2, CORES, erow, fx)
        for k in both(i):
            spread(hid_part, hx_s, hx_r, k)

    def step_f(i):
        for k in both(i):
            with jax.named_scope(f"f_relay{k}"):
                relay(hid_part, hx_s, hx_r, k)

    def step_g(i):
        for k in both(i):
            with jax.named_scope(f"g_settle{k}"):
                settle(hid_part, hx_s, hx_r, k)
        if i == 0:
            weights[2].wait()
        with jax.named_scope(f"g_dot{i}"):
            rows = hid[2 * i : 2 * i + 2].reshape(2 * CORES * erow, hid.shape[3])
            part = jnp.dot(rows, w_dn[...], preferred_element_type=f32)
            part = part.reshape(2, CORES, erow, dx)
            acc[...] = part
            psend[2 * i : 2 * i + 2] = part.astype(bf16)
        two = pl.ds(2 * i, 2)
        pending["g", i] = begin(
            remote(psend.at[two, 1 - c], precv.at[two], pc_s.at[i], pc_r.at[i], partner)
        )

    def step_i(i):
        with jax.named_scope(f"i_wait{i}"):
            pending["g", i].wait_recv()
        total = acc[:, c] + precv[2 * i : 2 * i + 2].astype(f32)
        half[i] = total
        qsend[2 * i : 2 * i + 2] = total.astype(bf16)
        pending["i", i] = begin(
            remote(qsend.at[2 * i + 1 - h], qrecv.at[i], qy_s.at[i], qy_r.at[i], mate)
        )

    def step_j(i):
        with jax.named_scope(f"j_wait{i}"):
            pending["i", i].wait_recv()
        done = (half[i, h] + qrecv[i].astype(f32)).astype(bf16)
        if i == 0:
            yback[0] = done
            return
        fsend[i] = done
        back = lax.rem(y + ys_n + hops[i] * (2 * h - 1), ys_n)
        pending["j", i] = begin(
            remote(fsend.at[i], yback.at[i], fy_s.at[i], fy_r.at[i], at(z, back, c, x))
        )

    def z_return(group):
        if group == 0:
            perm = unpermutation(mates * erow, b_slots, brow)
        else:
            perm = unpermutation(erow, a_slots, arow)
        with jax.named_scope(f"back_wait{group}"):
            for i in range(1, mates) if group == 0 else (mates,):
                pending["j", i].wait_recv()
        if group == 0:
            rows = yback[0:mates].reshape(mates * erow, dx)
            send, got, ss, rs = zback_a, zgot_a, zb_s, zb_r
        else:
            rows = yback[mates]
            send, got, ss, rs = zback_b, zgot_b, zc_s, zc_r
        moved = jnp.dot(perm, rows, preferred_element_type=f32).astype(bf16)
        send[...] = moved.reshape(send.shape)
        kept = []
        for r in near:
            zt = zpeer(r)
            copy = remote(send.at[zt], got.at[z], ss.at[r], rs.at[r], at(zt, y, c, x))
            copy.start()
            kept.append(copy)
        got[z] = send[z]
        backs_z.extend(kept)
        return kept

    def branch_core():
        with jax.named_scope("bz_wait"):
            for copy in bz:
                copy.wait_recv()
        begin(remote(bw.at[:, :, :, c], bw.at[:, :, :, c], bc_s.at[0], bc_r.at[0], partner))

    def branch_dense():
        ref = bw.at[:, :, :, 1 - c]
        remote(ref, ref, bc_s.at[0], bc_r.at[0], partner).wait_recv()
        whole_in = bw[0].reshape(width, bw.shape[5])
        pre = jnp.dot(normed[...], whole_in, preferred_element_type=f32)
        hb = (pre / (1.0 + jnp.exp(-pre))).astype(bf16)
        for xx in range(xs_n):
            zpart = zs_n // xs_n if zs_n >= xs_n else 0
            if zpart:
                wo = bw[1, xx * zpart : (xx + 1) * zpart].reshape(dx, bw.shape[5])
            else:
                wo = bw[1].reshape(width, bw.shape[5])[xx * dx : (xx + 1) * dx]
            term = lax.dot_general(hb, wo, (((1,), (1,)), ((), ())), preferred_element_type=f32)
            bterm[xx] = term.astype(bf16)

    def branch_send():
        for r in range(1, xs_n):
            xt = xpeer(r)
            copy = remote(bterm.at[xt], bgot.at[r], bx_s.at[r], bx_r.at[r], at(z, y, c, xt))
            copy.start()
            bx.append(copy)

    last = pairs - 1
    own_pair()
    other_pairs()
    step_b(0)
    step_c(0)
    branch_planes()
    step_e(0)
    if pairs == 4:
        order = ("a1", "f0", "b1", "a2", "g0", "c1", "a3", "i0", "e1", "b2", "j0", "core", "b3", "c2", "e2", "f1", "c3", "e3", "dense", "g1", "f2", "i1", "j1", "f3", "g2", "i2", "g3", "send", "j2", "i3")
    else:
        order = ("a1", "f0", "b1", "g0", "c1", "i0", "e1", "j0", "core", "dense", "f1", "g1", "send", "i1")
    steps = dict(a=step_a, b=step_b, c=step_c, e=step_e, f=step_f, g=step_g, i=step_i, j=step_j)
    others = dict(core=branch_core, dense=branch_dense, send=branch_send)
    for item in order:
        if item in others:
            others[item]()
        else:
            steps[item[0]](int(item[1]))
    step_j(last)
    kept_a = z_return(0)
    kept_b = z_return(1)

    diff = scores_t[0:1, :] - scores_t[1:2, :]
    mixes = []
    for d in (diff, -diff):
        row = jnp.broadcast_to(sigmoid(d), sq)
        mixes.append(jnp.sum(jnp.where(sq_a == sq_b, row, 0.0), axis=1, keepdims=True))

    def combine(low, slots, got):
        t = lax.broadcasted_iota(jnp.int32, (slots, rows_tok), 0).astype(f32) + low
        rows = got[...].reshape(slots, dx)
        total = None
        for r in (0, 1):
            g = jnp.where(t == come[r], 1.0, 0.0).astype(bf16)
            term = lax.dot_general(g, rows, (((0,), (0,)), ((), ())), preferred_element_type=f32)
            total = mixes[r] * term if total is None else total + mixes[r] * term
        return total

    with jax.named_scope("bx_wait"):
        for copy in bx:
            copy.wait_recv()
    share = bterm[x].astype(f32)
    for r in range(1, xs_n):
        share = share + bgot[r].astype(f32)
    share = share * branch_weight
    with jax.named_scope("kept_a"):
        for copy in kept_a:
            copy.wait_recv()
    share = share + combine(0.0, b_slots, zgot_a)
    with jax.named_scope("kept_b"):
        for copy in kept_b:
            copy.wait_recv()
    out[...] = (share + combine(b_slots * 1.0, a_slots, zgot_b)).astype(out.dtype)

    with jax.named_scope("send_wait"):
        for copy in zd + by + bz + started + bx + backs_z:
            copy.wait_send()


def on_device(
    cores_z,
    cores_y,
    tokens,
    norm_gain,
    routes,
    route_scores,
    expert_gate,
    expert_up,
    expert_down,
    branch_in,
    branch_out,
    branch_gate,
):
    zs_n, ys_n = cores_z, cores_y
    xs_n = lax.axis_size("tp")
    rows_tok, width = tokens.shape
    experts = zs_n * ys_n // 2
    cap = 5 * rows_tok * routes.shape[1] // (4 * experts)
    pairs = ys_n // 2
    dx = width // xs_n
    fx = expert_gate.shape[2]
    fg = expert_down.shape[1]
    arow = round_up(cap, 16)
    brow = round_up((pairs - 1) * cap, 16)
    erow = round_up(zs_n * cap, 16)
    bpart = branch_in.shape
    bf16, f32 = jnp.bfloat16, jnp.float32
    vm = lambda shape, dtype=bf16: pltpu.VMEM(shape, dtype)
    sem = lambda *shape: pltpu.SemaphoreType.DMA(shape)
    scratch = [
        vm((rows_tok, width)),
        vm((zs_n, arow, dx)),
        vm((zs_n, brow, dx)),
        vm((zs_n, arow, dx)),
        vm((zs_n, brow, dx)),
        vm((pairs - 1, erow, dx)),
        vm((ys_n, CORES, erow, width)),
        vm((width, 2 * fx)),
        vm((fg, dx)),
        vm((ys_n, CORES, erow, fg)),
        vm((2, CORES, erow, dx), f32),
        vm((ys_n, CORES, erow, dx)),
        vm((ys_n, erow, dx)),
        vm((pairs, 2, erow, dx), f32),
        vm((ys_n, erow, dx)),
        vm((pairs, erow, dx)),
        vm((pairs, erow, dx)),
        vm((pairs, erow, dx)),
        vm((zs_n, brow, dx)),
        vm((zs_n, arow, dx)),
        vm((zs_n, brow, dx)),
        vm((zs_n, arow, dx)),
        vm((2, zs_n, ys_n, CORES, *bpart)),
        vm((xs_n, rows_tok, dx)),
        vm((xs_n, rows_tok, dx)),
        sem(3),
        sem(zs_n),
        sem(zs_n),
        sem(zs_n),
        sem(zs_n),
        sem(ys_n),
        sem(ys_n),
        sem(3, ys_n),
        sem(3, ys_n),
        sem(ys_n),
        sem(ys_n),
        sem(3, ys_n),
        sem(3, ys_n),
        sem(pairs),
        sem(pairs),
        sem(pairs),
        sem(pairs),
        sem(pairs),
        sem(pairs),
        sem(zs_n),
        sem(zs_n),
        sem(zs_n),
        sem(zs_n),
        sem(2, ys_n),
        sem(2, ys_n),
        sem(zs_n),
        sem(zs_n),
        sem(1),
        sem(1),
        sem(xs_n),
        sem(xs_n),
    ]
    in_vmem = pl.BlockSpec(memory_space=pltpu.VMEM)
    in_hbm = pl.BlockSpec(memory_space=pl.ANY)
    return pl.pallas_call(
        functools.partial(layer_kernel, zs_n, ys_n, xs_n, cap),
        out_shape=jax.ShapeDtypeStruct((rows_tok, dx), bf16),
        in_specs=[in_vmem] * 7 + [in_hbm] * 3,
        out_specs=in_vmem,
        scratch_shapes=scratch,
        compiler_params=pltpu.CompilerParams(
            collective_id=0, has_side_effects=True, vmem_limit_bytes=60 * 1024 * 1024
        ),
        name="routed_layer",
    )(
        tokens,
        norm_gain.reshape(1, -1),
        routes.T,
        route_scores.T,
        branch_gate.reshape(1, -1),
        branch_in,
        branch_out.T,
        expert_gate,
        expert_up,
        expert_down,
    )


def solution(mesh, z_y=None):
    ep = mesh.shape["ep"]
    zs_n, ys_n = z_y or (8, ep // (8 * CORES))
    in_specs = (
        P("ep", None),
        P(),
        P("ep", None),
        P("ep", None),
        P("ep", None, "tp"),
        P("ep", None, "tp"),
        P("ep", None, "tp"),
        P("ep", "tp"),
        P("tp", "ep"),
        P(),
    )
    return jax.shard_map(
        functools.partial(on_device, zs_n, ys_n),
        mesh=mesh,
        in_specs=in_specs,
        out_specs=P("ep", "tp"),
        check_vma=False,
    )
```

time: 134 us -> 105 us (0.78); the launches traced: 132 us -> 105 us
  Pallas kernels: 127 us -> 104 us
  local copies, waits for them, and re-layouts: 3.83 us -> 1.57 us
    pallas_call x1, Pallas kernels: 127 us -> 104 us  [on_device(): pl.pallas_call(functools.partial(layer_kernel, zs_n, ys_n, xs_n, cap), ou...]
    unnamed x11 -> x1, local copies, waits for them, and re-layouts: 3.83 us -> 1.57 us
where the time goes in v2:
time: 105 us
  Pallas kernels  104 us (99%)
  local copies, waits for them, and re-layouts  1.57 us (1%)
    pallas_call x1, Pallas kernels, on_device(): pl.pallas_call(functools.partial(layer_kernel, zs_n, ys_n, xs_n, cap), ou...  104 us

profile of v2, /device:TPU:1, one launch (start us, length us, event | category | flops | bytes accessed | tf_op | source)
XLA Modules:
  0.0 105.3 jit_solution(8829469261477574202)
XLA Ops:
  0.0 103.7 %routed_layer.1 = bf16[128,512]{1,0:T(8,128)(2,1)} custom-call(bf16[128,2048]{1,0:T(8,128)(2,1)} %tokens.1, f32[1,2048]{1,0:T(1,128)} %bitcast.5, s32[2,128]{1,0:T(2,128)} %bitcast.8, f32[2,128]{1,0:T(2,128)} %bitcast.9, f32[1,2048]{1,0:T(1,128)} %bitcast.6, bf16[16,128]{1,0:T(8,128)(2,1)} %b_in.1, bf16[16,128]{1,0:T(8,128)(2,1)} %bitcast.7, ...), custom_call_target="tpu_custom_call" | custom-call | tf_op jit(solution)/shard_map/routed_layer/pallas_call | solution.py:604
  103.7 1.6 %copy.12 = bf16[128,512]{1,0:T(8,128)(2,1)} copy(bf16[128,512]{1,0:T(8,128)(2,1)} %routed_layer.1) | data formatting | bytes 262144

commit v3 on v2

--- a/solution.py
+++ b/solution.py
@@ -23,6 +23,10 @@
 
 def floor_div(v, n):
     return jnp.floor((v + 0.5) * (1.0 / n))
+
+
+def return_groups(pairs):
+    return [[0, 1], [2], [3]] if pairs == 4 else [[i] for i in range(pairs)]
 
 
 def layer_kernel(
@@ -55,14 +59,11 @@
     psend,
     precv,
     half,
-    qsend,
     qrecv,
     fsend,
     yback,
-    zback_a,
-    zback_b,
-    zgot_a,
-    zgot_b,
+    zback,
+    zgot,
     bw,
     bterm,
     bgot,
@@ -87,8 +88,6 @@
     fy_r,
     zb_s,
     zb_r,
-    zc_s,
-    zc_r,
     by_s,
     by_r,
     bz_s,
@@ -117,6 +116,10 @@
     a_slots, b_slots = zs_n * arow, zs_n * brow
     erow = ysend.shape[1]
     mates = pairs - 1
+    far = hops.index(pairs - 1)
+    groups = return_groups(pairs)
+    g_rows = [round_up(len(g) * cap, 16) for g in groups]
+    g_low = [zs_n * sum(g_rows[:n]) for n in range(len(groups))]
 
     def at(z_, y_, c_, x_):
         return ((z_ * ys_n + y_) * CORES + c_, x_)
@@ -174,10 +177,11 @@
             rank
             + jnp.where(rel < 0.5, zz * arow, a_slots + zz * brow + (rel - 1.0) * cap)
         )
-        come.append(
-            rank
-            + jnp.where(rel < mates - 0.5, zz * brow + rel * cap, b_slots + zz * arow)
-        )
+        place = 0.0
+        for group, n_rows, low in zip(groups, g_rows, g_low):
+            spot = low + zz * n_rows + (rel - group[0]) * cap
+            place = spot if group[0] == 0 else jnp.where(rel > group[0] - 0.5, spot, place)
+        come.append(rank + place)
     srow = lax.broadcasted_iota(jnp.int32, (a_slots + b_slots, rows_tok), 0).astype(f32)
     pick = jnp.where((srow == go[0]) | (srow == go[1]), 1.0, 0.0).astype(bf16)
     own_cols = pl.ds(pl.multiple_of(x * dx, dx), dx)
@@ -234,7 +238,7 @@
     east, west = at(z, y, c, xpeer(1)), at(z, y, c, xpeer(xs_n - 1))
     partner = at(z, y, 1 - c, x)
     mate = at(z, y + 1 - 2 * h, c, x)
-    started, backs, bz, bx, backs_z = [], [], [], [], []
+    started, bz, bx, backs_z, returned = [], [], [], [], []
     pending = {}
 
     def begin(copy):
@@ -297,12 +301,15 @@
         for i in range(1, pairs):
             pt = lax.rem(pair + pairs + i * (1 - 2 * h), pairs)
             k = 2 * i + lax.rem(h + hops[i], 2)
-            for hh in (0, 1):
+            near_chip = lax.rem(h + hops[i], 2)
+            for n, hh in enumerate((near_chip, 1 - near_chip)):
+                if i == far and n == 1:
+                    break
                 begin(
                     remote(
                         ysend.at[i - 1],
                         tok.at[k, c, :, own_cols],
-                        yd_s.at[2 * i + hh],
+                        yd_s.at[2 * i + n],
                         yd_r.at[k],
                         at(z, 2 * pt + hh, c, x),
                     )
@@ -317,11 +324,27 @@
             copy.start()
             bz.append(copy)
 
+    def step_k(k):
+        with jax.named_scope(f"a_wait{k}"):
+            y_wait(k)
+        spread(tok_part, tx_s, tx_r, k)
+
     def step_a(i):
         for k in both(i):
-            with jax.named_scope(f"a_wait{k}"):
-                y_wait(k)
-            spread(tok_part, tx_s, tx_r, k)
+            step_k(k)
+
+    def step_n(i):
+        mine = 2 * i + h
+        with jax.named_scope(f"far_wait{i}"):
+            y_wait(mine)
+        ref = tok.at[mine, c, :, own_cols]
+        begin(remote(ref, ref, yd_s.at[2 * i + 1], yd_r.at[mine], mate))
+        spread(tok_part, tx_s, tx_r, mine)
+
+    def step_m(i):
+        with jax.named_scope(f"far_mate{i}"):
+            y_wait(2 * i + 1 - h)
+        spread(tok_part, tx_s, tx_r, 2 * i + 1 - h)
 
     def step_b(i):
         for k in both(i):
@@ -379,50 +402,65 @@
         with jax.named_scope(f"i_wait{i}"):
             pending["g", i].wait_recv()
         total = acc[:, c] + precv[2 * i : 2 * i + 2].astype(f32)
-        half[i] = total
-        qsend[2 * i : 2 * i + 2] = total.astype(bf16)
-        pending["i", i] = begin(
-            remote(qsend.at[2 * i + 1 - h], qrecv.at[i], qy_s.at[i], qy_r.at[i], mate)
-        )
+        fsend[2 * i : 2 * i + 2] = total.astype(bf16)
+        if i == 0:
+            yback[0, h] = fsend[h]
+            begin(remote(fsend.at[1 - h], yback.at[0, h], fy_s.at[0], fy_r.at[0, h], mate))
+            return
+        if i == far:
+            half[...] = total
+            copy = remote(fsend.at[2 * i + 1 - h], qrecv, qy_s.at[0], qy_r.at[0], mate)
+            pending["i", i] = begin(copy)
+            return
+        for side in (0, 1):
+            way = hops[i] + 1 if side else ys_n - hops[i]
+            back = at(z, lax.rem(2 * pair + way, ys_n), c, x)
+            k = 2 * i + side
+            begin(remote(fsend.at[k], yback.at[i, h], fy_s.at[k], fy_r.at[i, h], back))
 
     def step_j(i):
         with jax.named_scope(f"j_wait{i}"):
             pending["i", i].wait_recv()
-        done = (half[i, h] + qrecv[i].astype(f32)).astype(bf16)
-        if i == 0:
-            yback[0] = done
-            return
-        fsend[i] = done
-        back = lax.rem(y + ys_n + hops[i] * (2 * h - 1), ys_n)
-        pending["j", i] = begin(
-            remote(fsend.at[i], yback.at[i], fy_s.at[i], fy_r.at[i], at(z, back, c, x))
-        )
-
-    def z_return(group):
-        if group == 0:
-            perm = unpermutation(mates * erow, b_slots, brow)
-        else:
-            perm = unpermutation(erow, a_slots, arow)
-        with jax.named_scope(f"back_wait{group}"):
-            for i in range(1, mates) if group == 0 else (mates,):
-                pending["j", i].wait_recv()
-        if group == 0:
-            rows = yback[0:mates].reshape(mates * erow, dx)
-            send, got, ss, rs = zback_a, zgot_a, zb_s, zb_r
-        else:
-            rows = yback[mates]
-            send, got, ss, rs = zback_b, zgot_b, zc_s, zc_r
-        moved = jnp.dot(perm, rows, preferred_element_type=f32).astype(bf16)
-        send[...] = moved.reshape(send.shape)
+        fsend[2 * i + h] = (half[h] + qrecv[...].astype(f32)).astype(bf16)
+        back = at(z, lax.rem(y + ys_n + hops[i] * (2 * h - 1), ys_n), c, x)
+        k = 2 * i + h
+        begin(remote(fsend.at[k], yback.at[i, 0], fy_s.at[2 * i], fy_r.at[i, 0], back))
+
+    def back_wait(i, hh):
+        ref = yback.at[i, hh]
+        remote(ref, ref, fy_s.at[0], fy_r.at[i, hh], mate).wait_recv()
+
+    def z_return(n):
+        group, step = groups[n], g_rows[n]
+        many, slots = len(group) * erow, zs_n * step
+        perm = unpermutation(many, slots, step)
+        with jax.named_scope(f"back_wait{n}"):
+            for i in group:
+                if i == 0:
+                    back_wait(0, 1 - h)
+                elif i == far:
+                    back_wait(i, 0)
+                else:
+                    back_wait(i, 0)
+                    back_wait(i, 1)
+        moved = 0.0
+        for hh in (0,) if group == [far] else (0, 1):
+            rows = yback[group[0] : group[-1] + 1, hh].reshape(many, dx)
+            moved = moved + jnp.dot(perm, rows, preferred_element_type=f32)
+        base = sum(g_rows[:n])
+        zback[:, base : base + step] = moved.astype(bf16).reshape(zs_n, step, dx)
+        rows = pl.ds(base, step)
         kept = []
         for r in near:
             zt = zpeer(r)
-            copy = remote(send.at[zt], got.at[z], ss.at[r], rs.at[r], at(zt, y, c, x))
+            copy = remote(
+                zback.at[zt, rows], zgot.at[z, rows], zb_s.at[n, r], zb_r.at[n, r], at(zt, y, c, x)
+            )
             copy.start()
             kept.append(copy)
-        got[z] = send[z]
+        zgot[z, base : base + step] = zback[z, base : base + step]
         backs_z.extend(kept)
-        return kept
+        returned.append((n, kept))
 
     def branch_core():
         with jax.named_scope("bz_wait"):
@@ -452,27 +490,20 @@
             copy.start()
             bx.append(copy)
 
-    last = pairs - 1
     own_pair()
     other_pairs()
-    step_b(0)
-    step_c(0)
-    branch_planes()
-    step_e(0)
     if pairs == 4:
-        order = ("a1", "f0", "b1", "a2", "g0", "c1", "a3", "i0", "e1", "b2", "j0", "core", "b3", "c2", "e2", "f1", "c3", "e3", "dense", "g1", "f2", "i1", "j1", "f3", "g2", "i2", "g3", "send", "j2", "i3")
+        order = ("b0", "k2", "c0", "planes", "e0", "k3", "n2", "f0", "b1", "m2", "a3", "g0", "c1", "b2", "i0", "e1", "core", "b3", "c2", "e2", "c3", "f1", "e3", "g1", "f2", "i1", "f3", "dense", "g2", "i2", "g3", "send", "z0", "i3", "j2", "z2", "z1")
     else:
-        order = ("a1", "f0", "b1", "g0", "c1", "i0", "e1", "j0", "core", "dense", "f1", "g1", "send", "i1")
+        order = ("b0", "n1", "m1", "c0", "planes", "e0", "f0", "b1", "g0", "c1", "i0", "e1", "core", "dense", "f1", "g1", "send", "i1", "j1", "z0", "z1")
     steps = dict(a=step_a, b=step_b, c=step_c, e=step_e, f=step_f, g=step_g, i=step_i, j=step_j)
-    others = dict(core=branch_core, dense=branch_dense, send=branch_send)
+    steps.update(k=step_k, z=z_return, n=step_n, m=step_m)
+    others = dict(planes=branch_planes, core=branch_core, dense=branch_dense, send=branch_send)
     for item in order:
         if item in others:
             others[item]()
         else:
             steps[item[0]](int(item[1]))
-    step_j(last)
-    kept_a = z_return(0)
-    kept_b = z_return(1)
 
     diff = scores_t[0:1, :] - scores_t[1:2, :]
     mixes = []
@@ -480,9 +511,11 @@
         row = jnp.broadcast_to(sigmoid(d), sq)
         mixes.append(jnp.sum(jnp.where(sq_a == sq_b, row, 0.0), axis=1, keepdims=True))
 
-    def combine(low, slots, got):
-        t = lax.broadcasted_iota(jnp.int32, (slots, rows_tok), 0).astype(f32) + low
-        rows = got[...].reshape(slots, dx)
+    def combine(n):
+        slots = zs_n * g_rows[n]
+        base = sum(g_rows[:n])
+        t = lax.broadcasted_iota(jnp.int32, (slots, rows_tok), 0).astype(f32) + 1.0 * g_low[n]
+        rows = zgot[:, base : base + g_rows[n]].reshape(slots, dx)
         total = None
         for r in (0, 1):
             g = jnp.where(t == come[r], 1.0, 0.0).astype(bf16)
@@ -497,14 +530,12 @@
     for r in range(1, xs_n):
         share = share + bgot[r].astype(f32)
     share = share * branch_weight
-    with jax.named_scope("kept_a"):
-        for copy in kept_a:
-            copy.wait_recv()
-    share = share + combine(0.0, b_slots, zgot_a)
-    with jax.named_scope("kept_b"):
-        for copy in kept_b:
-            copy.wait_recv()
-    out[...] = (share + combine(b_slots * 1.0, a_slots, zgot_b)).astype(out.dtype)
+    for n, kept in returned:
+        with jax.named_scope(f"kept{n}"):
+            for copy in kept:
+                copy.wait_recv()
+        share = share + combine(n)
+    out[...] = share.astype(out.dtype)
 
     with jax.named_scope("send_wait"):
         for copy in zd + by + bz + started + bx + backs_z:
@@ -537,6 +568,7 @@
     arow = round_up(cap, 16)
     brow = round_up((pairs - 1) * cap, 16)
     erow = round_up(zs_n * cap, 16)
+    back_rows = sum(round_up(len(g) * cap, 16) for g in return_groups(pairs))
     bpart = branch_in.shape
     bf16, f32 = jnp.bfloat16, jnp.float32
     vm = lambda shape, dtype=bf16: pltpu.VMEM(shape, dtype)
@@ -555,15 +587,12 @@
         vm((2, CORES, erow, dx), f32),
         vm((ys_n, CORES, erow, dx)),
         vm((ys_n, erow, dx)),
-        vm((pairs, 2, erow, dx), f32),
+        vm((2, erow, dx), f32),
+        vm((erow, dx)),
         vm((ys_n, erow, dx)),
-        vm((pairs, erow, dx)),
-        vm((pairs, erow, dx)),
-        vm((pairs, erow, dx)),
-        vm((zs_n, brow, dx)),
-        vm((zs_n, arow, dx)),
-        vm((zs_n, brow, dx)),
-        vm((zs_n, arow, dx)),
+        vm((pairs, 2, erow, dx)),
+        vm((zs_n, back_rows, dx)),
+        vm((zs_n, back_rows, dx)),
         vm((2, zs_n, ys_n, CORES, *bpart)),
         vm((xs_n, rows_tok, dx)),
         vm((xs_n, rows_tok, dx)),
@@ -582,14 +611,12 @@
         sem(3, ys_n),
         sem(pairs),
         sem(pairs),
-        sem(pairs),
-        sem(pairs),
-        sem(pairs),
-        sem(pairs),
-        sem(zs_n),
-        sem(zs_n),
-        sem(zs_n),
-        sem(zs_n),
+        sem(1),
+        sem(1),
+        sem(ys_n),
+        sem(pairs, 2),
+        sem(pairs, zs_n),
+        sem(pairs, zs_n),
         sem(2, ys_n),
         sem(2, ys_n),
         sem(zs_n),

time: 105 us -> 97.8 us (0.931)
  Pallas kernels: 104 us -> 96.1 us
    pallas_call x1, Pallas kernels: 104 us -> 96.1 us  [on_device(): pl.pallas_call(functools.partial(layer_kernel, zs_n, ys_n, xs_n, cap), ou...]
where the time goes in v3:
time: 97.8 us; the launch traced here: 97.6 us
  Pallas kernels  96.1 us (98%)
  local copies, waits for them, and re-layouts  1.57 us (2%)
    pallas_call x1, Pallas kernels, on_device(): pl.pallas_call(functools.partial(layer_kernel, zs_n, ys_n, xs_n, cap), ou...  96.1 us

profile of v3, /device:TPU:1, one launch (start us, length us, event | category | flops | bytes accessed | tf_op | source)
XLA Modules:
  0.0 97.6 jit_solution(8596398432811432472)
XLA Ops:
  0.0 96.1 %routed_layer.1 = bf16[128,512]{1,0:T(8,128)(2,1)} custom-call(bf16[128,2048]{1,0:T(8,128)(2,1)} %tokens.1, f32[1,2048]{1,0:T(1,128)} %bitcast.5, s32[2,128]{1,0:T(2,128)} %bitcast.8, f32[2,128]{1,0:T(2,128)} %bitcast.9, f32[1,2048]{1,0:T(1,128)} %bitcast.6, bf16[16,128]{1,0:T(8,128)(2,1)} %b_in.1, bf16[16,128]{1,0:T(8,128)(2,1)} %bitcast.7, ...), custom_call_target="tpu_custom_call" | custom-call | tf_op jit(solution)/shard_map/routed_layer/pallas_call | solution.py:631
  96.1 1.6 %copy.12 = bf16[128,512]{1,0:T(8,128)(2,1)} copy(bf16[128,512]{1,0:T(8,128)(2,1)} %routed_layer.1) | data formatting | bytes 262144

commit v4 on v3

--- a/solution.py
+++ b/solution.py
@@ -46,10 +46,10 @@
     w_down,
     out,
     normed,
-    zsend_a,
-    zsend_b,
-    zrecv_a,
-    zrecv_b,
+    zsend,
+    zrecv,
+    wsend,
+    wrecv,
     ysend,
     tok,
     w_gu,
@@ -68,8 +68,6 @@
     bterm,
     bgot,
     local_sem,
-    za_s,
-    za_r,
     zd_s,
     zd_r,
     yd_s,
@@ -106,17 +104,17 @@
     pairs = ys_n // 2
     pair = y // 2
     h = lax.rem(y, 2)
-    hops = [0] + list(range(2, pairs)) + [1]
+    hops = list(range(1, pairs)) + [0]
+    last = pairs - 1
+    offset = [last] + list(range(1, last)) + [0]
     rows_tok, width = tokens.shape
     dx = width // xs_n
     fx = w_gate.shape[2]
     experts = zs_n * pairs
-    arow = zsend_a.shape[1]
-    brow = zsend_b.shape[1]
-    a_slots, b_slots = zs_n * arow, zs_n * brow
+    arow = zsend.shape[2]
+    slots = zs_n * arow
     erow = ysend.shape[1]
-    mates = pairs - 1
-    far = hops.index(pairs - 1)
+    far = hops.index(last)
     groups = return_groups(pairs)
     g_rows = [round_up(len(g) * cap, 16) for g in groups]
     g_low = [zs_n * sum(g_rows[:n]) for n in range(len(groups))]
@@ -173,48 +171,56 @@
         zz = floor_div(e, pairs)
         v = (e - zz * pairs - pair.astype(f32)) * (1 - 2 * h).astype(f32) + pairs
         rel = jnp.where(v >= pairs, v - pairs, v)
-        go.append(
-            rank
-            + jnp.where(rel < 0.5, zz * arow, a_slots + zz * brow + (rel - 1.0) * cap)
-        )
+        rel = jnp.where(rel < 0.5, 1.0 * last, jnp.where(rel > last - 0.5, 0.0, rel))
+        go.append(rank + rel * slots + zz * arow)
         place = 0.0
         for group, n_rows, low in zip(groups, g_rows, g_low):
             spot = low + zz * n_rows + (rel - group[0]) * cap
             place = spot if group[0] == 0 else jnp.where(rel > group[0] - 0.5, spot, place)
         come.append(rank + place)
-    srow = lax.broadcasted_iota(jnp.int32, (a_slots + b_slots, rows_tok), 0).astype(f32)
+    srow = lax.broadcasted_iota(jnp.int32, (pairs * slots, rows_tok), 0).astype(f32)
     pick = jnp.where((srow == go[0]) | (srow == go[1]), 1.0, 0.0).astype(bf16)
     own_cols = pl.ds(pl.multiple_of(x * dx, dx), dx)
-    packed = jnp.dot(pick, normed[:, own_cols], preferred_element_type=f32).astype(bf16)
-    zsend_a[...] = packed[:a_slots].reshape(zs_n, arow, dx)
-    zsend_b[...] = packed[a_slots:].reshape(zs_n, brow, dx)
+    packed = jnp.dot(pick[: last * slots], normed[:, own_cols], preferred_element_type=f32)
+    zsend[...] = packed.astype(bf16).reshape(last, zs_n, arow, dx)
 
     pl.semaphore_wait(barrier, len(peers))
 
-    za, zd, by = [], [], []
+    zd, by = {}, []
     near = sorted(range(1, zs_n), key=lambda r: min(r, zs_n - r))
-    for src, dst, ss, rs, kept in (
-        (zsend_a, zrecv_a, za_s, za_r, za),
-        (zsend_b, zrecv_b, zd_s, zd_r, zd),
-    ):
-        for copy in za:
-            copy.wait_send()
+
+    def z_send(i):
+        src, dst = (wsend, wrecv) if i == last else (zsend.at[i], zrecv.at[i])
+        zd[i] = []
         for r in near:
             zt = zpeer(r)
-            copy = remote(src.at[zt], dst.at[z], ss.at[r], rs.at[r], at(zt, y, c, x))
+            copy = remote(src.at[zt], dst.at[z], zd_s.at[i], zd_r.at[i], at(zt, y, c, x))
             copy.start()
-            kept.append(copy)
-    for r in range(1, ys_n):
+            zd[i].append(copy)
+
+    def zd_all(i):
+        ref = wrecv if i == last else zrecv.at[i]
+        ref = ref.at[pl.ds(0, zs_n - 1)]
+        return remote(ref, ref, zd_s.at[i], zd_r.at[i], at(z, y, 1 - c, x))
+
+    z_send(0)
+    for i in range(last):
+        zrecv[i, z] = zsend[i, z]
+    wide = jnp.dot(pick[last * slots :], normed[...], preferred_element_type=f32)
+    wsend[...] = wide.astype(bf16).reshape(zs_n, arow, width)
+    wrecv[z] = wsend[z]
+    if near:
+        zd_all(0).wait_send()
+    z_send(1)
+    for r in near:
         for w, part in enumerate((b_in, b_out)):
             copy = remote(
-                part, bw.at[w, z, y, c], by_s.at[w, r], by_r.at[w, r], at(z, ypeer(r), c, x)
+                part, bw.at[w, z, y, c], by_s.at[0], by_r.at[0], at(zpeer(r), y, c, x)
             )
             copy.start()
             by.append(copy)
     bw[0, z, y, c] = b_in[...]
     bw[1, z, y, c] = b_out[...]
-    zrecv_a[z] = zsend_a[z]
-    zrecv_b[z] = zsend_b[z]
 
     bsum = jnp.sum(normed[...].astype(f32) * bgate[...], axis=-1, keepdims=True)
     branch_weight = sigmoid(bsum)
@@ -254,17 +260,18 @@
 
     def spread(part, sems, rsems, k):
         for way, dev in ((0, east), (1, west)):
-            begin(remote(part(k, x), part(k, x), sems.at[way, k], rsems.at[way, k], dev))
+            begin(remote(part(k, x), part(k, x), sems.at[0], rsems.at[way, k], dev))
 
     def arrive(part, rsems, sems, way, k):
         ref = part(k, x)
-        remote(ref, ref, sems.at[way, k], rsems.at[way, k], east).wait_recv()
+        remote(ref, ref, sems.at[0], rsems.at[way, k], east).wait_recv()
 
     def relay(part, sems, rsems, k):
-        way = k % 2
+        way = lax.rem(k, 2)
         arrive(part, rsems, sems, way, k)
-        ref = part(k, xpeer(xs_n - 1) if way == 0 else xpeer(1))
-        begin(remote(ref, ref, sems.at[2, k], rsems.at[2, k], east if way == 0 else west))
+        ref = part(k, xpeer(xs_n - 1 - 2 * way))
+        dev = at(z, y, c, xpeer(1 + 2 * way))
+        begin(remote(ref, ref, sems.at[0], rsems.at[2, k], dev))
 
     def settle(part, sems, rsems, k):
         arrive(part, rsems, sems, 1 - k % 2, k)
@@ -277,95 +284,108 @@
     def both(i):
         return (2 * i, 2 * i + 1)
 
-    def own_pair():
-        with jax.named_scope("za_wait"):
-            for copy in za:
-                copy.wait_recv()
-        first = permutation(erow, a_slots, arow)
-        moved = jnp.dot(first, zrecv_a[...].reshape(a_slots, dx), preferred_element_type=f32)
-        tok[h, c, :, own_cols] = moved.astype(bf16)
-        ref = tok.at[h, c, :, own_cols]
-        begin(remote(ref, ref, yd_s.at[0], yd_r.at[h], mate))
-        spread(tok_part, tx_s, tx_r, h)
-        with jax.named_scope("y_wait_mate"):
-            y_wait(1 - h)
-        spread(tok_part, tx_s, tx_r, 1 - h)
-
-    def other_pairs():
-        rest = permutation(mates * erow, b_slots, brow)
-        with jax.named_scope("zb_wait"):
-            for copy in zd:
-                copy.wait_recv()
-        moved = jnp.dot(rest, zrecv_b[...].reshape(b_slots, dx), preferred_element_type=f32)
-        ysend[...] = moved.astype(bf16).reshape(mates, erow, dx)
-        for i in range(1, pairs):
-            pt = lax.rem(pair + pairs + i * (1 - 2 * h), pairs)
-            k = 2 * i + lax.rem(h + hops[i], 2)
-            near_chip = lax.rem(h + hops[i], 2)
-            for n, hh in enumerate((near_chip, 1 - near_chip)):
-                if i == far and n == 1:
-                    break
-                begin(
-                    remote(
-                        ysend.at[i - 1],
-                        tok.at[k, c, :, own_cols],
-                        yd_s.at[2 * i + n],
-                        yd_r.at[k],
-                        at(z, 2 * pt + hh, c, x),
-                    )
-                )
+    def step_d(i):
+        perm = permutation(erow, slots, arow)
+        with jax.named_scope(f"z_wait{i}"):
+            if near:
+                zd_all(i).wait_recv()
+        moved = jnp.dot(perm, zrecv[i].reshape(slots, dx), preferred_element_type=f32)
+        ysend[i] = moved.astype(bf16)
+        pt = lax.rem(pair + pairs + offset[i] * (1 - 2 * h), pairs)
+        near_chip = lax.rem(h + hops[i], 2)
+        k = 2 * i + near_chip
+        for n, hh in enumerate((near_chip, 1 - near_chip)):
+            if i == far and n == 1:
+                break
+            dst = tok.at[k, c, :, own_cols]
+            dev = at(z, 2 * pt + hh, c, x)
+            begin(remote(ysend.at[i], dst, yd_s.at[0], yd_r.at[k], dev))
+        if i + 2 <= last:
+            z_send(i + 2)
+
+    def to_partner(k, ref):
+        begin(remote(ref, ref, tc_s.at[0], tc_r.at[k], partner))
+
+    def step_o(part):
+        mine = 2 * last + h
+        if part == 1:
+            perm = permutation(erow, slots, arow)
+            with jax.named_scope("z_wait_wide"):
+                if near:
+                    zd_all(last).wait_recv()
+            moved = jnp.dot(perm, wrecv[...].reshape(slots, width), preferred_element_type=f32)
+            tok[mine, c] = moved.astype(bf16)
+            ref = tok.at[mine, c]
+            begin(remote(ref, ref, yd_s.at[0], yd_r.at[mine], mate))
+            to_partner(mine, ref)
+            return
+        ref = tok.at[2 * last + 1 - h, c]
+        with jax.named_scope("wide_mate"):
+            remote(ref, ref, yd_s.at[0], yd_r.at[2 * last + 1 - h], mate).wait_recv()
+        to_partner(2 * last + 1 - h, ref)
+
+    def by_all():
+        ref = bw.at[:, 0, pl.ds(0, zs_n - 1), 0]
+        return remote(ref, ref, by_s.at[0], by_r.at[0], partner)
+
+    def bz_all():
+        ref = bw.at[:, :, pl.ds(0, ys_n - 1), 0]
+        return remote(ref, ref, bz_s.at[0], bz_r.at[0], partner)
+
+    def bx_all():
+        ref = bgot.at[pl.ds(0, xs_n - 1)]
+        return remote(ref, ref, bx_s.at[0], bx_r.at[0], partner)
 
     def branch_planes():
-        for copy in by:
-            copy.wait_recv()
-        for r in range(1, zs_n):
-            part = bw.at[:, z, :, c]
-            copy = remote(part, part, bz_s.at[r], bz_r.at[r], at(zpeer(r), y, c, x))
+        if near:
+            by_all().wait_recv()
+        for r in range(1, ys_n):
+            part = bw.at[:, :, y, c]
+            copy = remote(part, part, bz_s.at[0], bz_r.at[0], at(z, ypeer(r), c, x))
             copy.start()
             bz.append(copy)
 
-    def step_k(k):
-        with jax.named_scope(f"a_wait{k}"):
-            y_wait(k)
-        spread(tok_part, tx_s, tx_r, k)
-
-    def step_a(i):
-        for k in both(i):
-            step_k(k)
-
     def step_n(i):
         mine = 2 * i + h
-        with jax.named_scope(f"far_wait{i}"):
+        with jax.named_scope(f"n_wait{i}"):
             y_wait(mine)
-        ref = tok.at[mine, c, :, own_cols]
-        begin(remote(ref, ref, yd_s.at[2 * i + 1], yd_r.at[mine], mate))
+        if i == far:
+            ref = tok.at[mine, c, :, own_cols]
+            begin(remote(ref, ref, yd_s.at[0], yd_r.at[mine], mate))
         spread(tok_part, tx_s, tx_r, mine)
+        to_partner(mine, tok_part(mine, x))
 
     def step_m(i):
-        with jax.named_scope(f"far_mate{i}"):
+        with jax.named_scope(f"m_wait{i}"):
             y_wait(2 * i + 1 - h)
-        spread(tok_part, tx_s, tx_r, 2 * i + 1 - h)
+        k = 2 * i + 1 - h
+        spread(tok_part, tx_s, tx_r, k)
+        to_partner(k, tok_part(k, x))
 
     def step_b(i):
-        for k in both(i):
-            with jax.named_scope(f"b_relay{k}"):
+        for n, k in enumerate((2 * i + h, 2 * i + 1 - h)):
+            with jax.named_scope(f"b_relay{i}_{n}"):
                 relay(tok_part, tx_s, tx_r, k)
+            to_partner(k, tok_part(k, xpeer(xs_n - 1 - 2 * lax.rem(k, 2))))
 
     def step_c(i):
         for k in both(i):
+            way = k % 2
             with jax.named_scope(f"c_settle{k}"):
-                settle(tok_part, tx_s, tx_r, k)
-            ref = tok.at[k, c]
-            begin(remote(ref, ref, tc_s.at[k], tc_r.at[k], partner))
+                arrive(tok_part, tx_r, tx_s, 1 - way, k)
+            to_partner(k, tok_part(k, xpeer(1 + 2 * way)))
+        for k in both(i):
+            with jax.named_scope(f"c_last{k}"):
+                arrive(tok_part, tx_r, tx_s, 2, k)
+            to_partner(k, tok_part(k, xpeer(2)))
 
     def step_e(i):
         with jax.named_scope(f"e_wait{i}"):
             for k in both(i):
                 ref = tok.at[k, 1 - c]
-                remote(ref, ref, tc_s.at[k], tc_r.at[k], partner).wait_recv()
-            if i == 0:
-                weights[0].wait()
-                weights[1].wait()
+                remote(ref, ref, tc_s.at[0], tc_r.at[k], partner).wait_recv()
+            while len(weights) > 1:
+                weights.pop(0).wait()
         with jax.named_scope(f"e_dot{i}"):
             rows = tok[2 * i : 2 * i + 2].reshape(2 * CORES * erow, width)
             pre = jnp.dot(rows, w_gu[...], preferred_element_type=f32)
@@ -385,8 +405,8 @@
         for k in both(i):
             with jax.named_scope(f"g_settle{k}"):
                 settle(hid_part, hx_s, hx_r, k)
-        if i == 0:
-            weights[2].wait()
+        while weights:
+            weights.pop(0).wait()
         with jax.named_scope(f"g_dot{i}"):
             rows = hid[2 * i : 2 * i + 2].reshape(2 * CORES * erow, hid.shape[3])
             part = jnp.dot(rows, w_dn[...], preferred_element_type=f32)
@@ -395,7 +415,7 @@
             psend[2 * i : 2 * i + 2] = part.astype(bf16)
         two = pl.ds(2 * i, 2)
         pending["g", i] = begin(
-            remote(psend.at[two, 1 - c], precv.at[two], pc_s.at[i], pc_r.at[i], partner)
+            remote(psend.at[two, 1 - c], precv.at[two], pc_s.at[0], pc_r.at[i], partner)
         )
 
     def step_i(i):
@@ -403,9 +423,10 @@
             pending["g", i].wait_recv()
         total = acc[:, c] + precv[2 * i : 2 * i + 2].astype(f32)
         fsend[2 * i : 2 * i + 2] = total.astype(bf16)
-        if i == 0:
-            yback[0, h] = fsend[h]
-            begin(remote(fsend.at[1 - h], yback.at[0, h], fy_s.at[0], fy_r.at[0, h], mate))
+        if i == last:
+            yback[i, h] = fsend[2 * i + h]
+            src = fsend.at[2 * i + 1 - h]
+            begin(remote(src, yback.at[i, h], fy_s.at[0], fy_r.at[i, h], mate))
             return
         if i == far:
             half[...] = total
@@ -416,7 +437,7 @@
             way = hops[i] + 1 if side else ys_n - hops[i]
             back = at(z, lax.rem(2 * pair + way, ys_n), c, x)
             k = 2 * i + side
-            begin(remote(fsend.at[k], yback.at[i, h], fy_s.at[k], fy_r.at[i, h], back))
+            begin(remote(fsend.at[k], yback.at[i, h], fy_s.at[0], fy_r.at[i, h], back))
 
     def step_j(i):
         with jax.named_scope(f"j_wait{i}"):
@@ -424,20 +445,25 @@
         fsend[2 * i + h] = (half[h] + qrecv[...].astype(f32)).astype(bf16)
         back = at(z, lax.rem(y + ys_n + hops[i] * (2 * h - 1), ys_n), c, x)
         k = 2 * i + h
-        begin(remote(fsend.at[k], yback.at[i, 0], fy_s.at[2 * i], fy_r.at[i, 0], back))
+        begin(remote(fsend.at[k], yback.at[i, 0], fy_s.at[0], fy_r.at[i, 0], back))
 
     def back_wait(i, hh):
         ref = yback.at[i, hh]
         remote(ref, ref, fy_s.at[0], fy_r.at[i, hh], mate).wait_recv()
 
+    def zb_all(n):
+        base = sum(g_rows[:n])
+        ref = zgot.at[pl.ds(0, zs_n - 1), pl.ds(base, g_rows[n])]
+        return remote(ref, ref, zb_s.at[n], zb_r.at[n], partner)
+
     def z_return(n):
         group, step = groups[n], g_rows[n]
-        many, slots = len(group) * erow, zs_n * step
-        perm = unpermutation(many, slots, step)
+        many = len(group) * erow
+        perm = unpermutation(many, zs_n * step, step)
         with jax.named_scope(f"back_wait{n}"):
             for i in group:
-                if i == 0:
-                    back_wait(0, 1 - h)
+                if i == last:
+                    back_wait(i, 1 - h)
                 elif i == far:
                     back_wait(i, 0)
                 else:
@@ -454,7 +480,7 @@
         for r in near:
             zt = zpeer(r)
             copy = remote(
-                zback.at[zt, rows], zgot.at[z, rows], zb_s.at[n, r], zb_r.at[n, r], at(zt, y, c, x)
+                zback.at[zt, rows], zgot.at[z, rows], zb_s.at[n], zb_r.at[n], at(zt, y, c, x)
             )
             copy.start()
             kept.append(copy)
@@ -464,8 +490,7 @@
 
     def branch_core():
         with jax.named_scope("bz_wait"):
-            for copy in bz:
-                copy.wait_recv()
+            bz_all().wait_recv()
         begin(remote(bw.at[:, :, :, c], bw.at[:, :, :, c], bc_s.at[0], bc_r.at[0], partner))
 
     def branch_dense():
@@ -486,18 +511,13 @@
     def branch_send():
         for r in range(1, xs_n):
             xt = xpeer(r)
-            copy = remote(bterm.at[xt], bgot.at[r], bx_s.at[r], bx_r.at[r], at(z, y, c, xt))
+            copy = remote(bterm.at[xt], bgot.at[r], bx_s.at[0], bx_r.at[0], at(z, y, c, xt))
             copy.start()
             bx.append(copy)
 
-    own_pair()
-    other_pairs()
-    if pairs == 4:
-        order = ("b0", "k2", "c0", "planes", "e0", "k3", "n2", "f0", "b1", "m2", "a3", "g0", "c1", "b2", "i0", "e1", "core", "b3", "c2", "e2", "c3", "f1", "e3", "g1", "f2", "i1", "f3", "dense", "g2", "i2", "g3", "send", "z0", "i3", "j2", "z2", "z1")
-    else:
-        order = ("b0", "n1", "m1", "c0", "planes", "e0", "f0", "b1", "g0", "c1", "i0", "e1", "core", "dense", "f1", "g1", "send", "i1", "j1", "z0", "z1")
-    steps = dict(a=step_a, b=step_b, c=step_c, e=step_e, f=step_f, g=step_g, i=step_i, j=step_j)
-    steps.update(k=step_k, z=z_return, n=step_n, m=step_m)
+    order = ("d0", "d1", "n0", "m0", "d2", "n1", "m1", "n2", "b1", "m2", "planes", "b0", "c1", "b2", "e1", "c0", "c2", "o1", "e0", "f1", "e2", "g1", "f0", "o2", "f2", "e3", "i1", "g0", "core", "i0", "g2", "i2", "f3", "z0", "dense", "j2", "g3", "i3", "send", "z2", "z1")
+    steps = dict(b=step_b, c=step_c, d=step_d, e=step_e, f=step_f, g=step_g, i=step_i, j=step_j)
+    steps.update(m=step_m, n=step_n, o=step_o, z=z_return)
     others = dict(planes=branch_planes, core=branch_core, dense=branch_dense, send=branch_send)
     for item in order:
         if item in others:
@@ -512,10 +532,10 @@
         mixes.append(jnp.sum(jnp.where(sq_a == sq_b, row, 0.0), axis=1, keepdims=True))
 
     def combine(n):
-        slots = zs_n * g_rows[n]
         base = sum(g_rows[:n])
-        t = lax.broadcasted_iota(jnp.int32, (slots, rows_tok), 0).astype(f32) + 1.0 * g_low[n]
-        rows = zgot[:, base : base + g_rows[n]].reshape(slots, dx)
+        shape = (zs_n * g_rows[n], rows_tok)
+        t = lax.broadcasted_iota(jnp.int32, shape, 0).astype(f32) + 1.0 * g_low[n]
+        rows = zgot[:, base : base + g_rows[n]].reshape(shape[0], dx)
         total = None
         for r in (0, 1):
             g = jnp.where(t == come[r], 1.0, 0.0).astype(bf16)
@@ -524,22 +544,39 @@
         return total
 
     with jax.named_scope("bx_wait"):
-        for copy in bx:
-            copy.wait_recv()
+        bx_all().wait_recv()
     share = bterm[x].astype(f32)
     for r in range(1, xs_n):
         share = share + bgot[r].astype(f32)
     share = share * branch_weight
     for n, kept in returned:
         with jax.named_scope(f"kept{n}"):
-            for copy in kept:
-                copy.wait_recv()
+            if near:
+                zb_all(n).wait_recv()
         share = share + combine(n)
     out[...] = share.astype(out.dtype)
 
     with jax.named_scope("send_wait"):
-        for copy in zd + by + bz + started + bx + backs_z:
-            copy.wait_send()
+        if near:
+            for i in range(1, pairs):
+                zd_all(i).wait_send()
+            for n in range(len(groups)):
+                zb_all(n).wait_send()
+            by_all().wait_send()
+        bz_all().wait_send()
+        bx_all().wait_send()
+        narrow = 2 * last
+        for ref, sem in (
+            (tok.at[pl.ds(0, last), :, :, pl.ds(0, 3 * dx)], tx_s),
+            (hid.at[:, :, :, pl.ds(0, 3 * fx)], hx_s),
+            (tok.at[:, 0], tc_s),
+            (tok.at[pl.ds(0, last + 2), :, :, pl.ds(0, dx)], yd_s),
+            (fsend.at[pl.ds(0, narrow)], fy_s),
+            (psend.at[:, 0], pc_s),
+            (qrecv, qy_s),
+            (bw.at[:, :, :, 0], bc_s),
+        ):
+            remote(ref, ref, sem.at[0], qy_r.at[0], partner).wait_send()
 
 
 def on_device(
@@ -566,7 +603,6 @@
     fx = expert_gate.shape[2]
     fg = expert_down.shape[1]
     arow = round_up(cap, 16)
-    brow = round_up((pairs - 1) * cap, 16)
     erow = round_up(zs_n * cap, 16)
     back_rows = sum(round_up(len(g) * cap, 16) for g in return_groups(pairs))
     bpart = branch_in.shape
@@ -575,10 +611,10 @@
     sem = lambda *shape: pltpu.SemaphoreType.DMA(shape)
     scratch = [
         vm((rows_tok, width)),
-        vm((zs_n, arow, dx)),
-        vm((zs_n, brow, dx)),
-        vm((zs_n, arow, dx)),
-        vm((zs_n, brow, dx)),
+        vm((pairs - 1, zs_n, arow, dx)),
+        vm((pairs - 1, zs_n, arow, dx)),
+        vm((zs_n, arow, width)),
+        vm((zs_n, arow, width)),
         vm((pairs - 1, erow, dx)),
         vm((ys_n, CORES, erow, width)),
         vm((width, 2 * fx)),
@@ -597,34 +633,32 @@
         vm((xs_n, rows_tok, dx)),
         vm((xs_n, rows_tok, dx)),
         sem(3),
-        sem(zs_n),
-        sem(zs_n),
-        sem(zs_n),
-        sem(zs_n),
-        sem(ys_n),
-        sem(ys_n),
-        sem(3, ys_n),
-        sem(3, ys_n),
-        sem(ys_n),
-        sem(ys_n),
-        sem(3, ys_n),
-        sem(3, ys_n),
         sem(pairs),
         sem(pairs),
         sem(1),
-        sem(1),
         sem(ys_n),
+        sem(1),
+        sem(3, ys_n),
+        sem(1),
+        sem(ys_n),
+        sem(1),
+        sem(3, ys_n),
+        sem(1),
+        sem(pairs),
+        sem(1),
+        sem(1),
+        sem(1),
         sem(pairs, 2),
-        sem(pairs, zs_n),
-        sem(pairs, zs_n),
-        sem(2, ys_n),
-        sem(2, ys_n),
-        sem(zs_n),
-        sem(zs_n),
-        sem(1),
-        sem(1),
-        sem(xs_n),
-        sem(xs_n),
+        sem(pairs),
+        sem(pairs),
+        sem(1),
+        sem(1),
+        sem(1),
+        sem(1),
+        sem(1),
+        sem(1),
+        sem(1),
+        sem(1),
     ]
     in_vmem = pl.BlockSpec(memory_space=pltpu.VMEM)
     in_hbm = pl.BlockSpec(memory_space=pl.ANY)

time: 97.8 us -> 93.2 us (0.953)
  Pallas kernels: 96.1 us -> 91.5 us
    pallas_call x1, Pallas kernels: 96.1 us -> 91.5 us  [on_device(): pl.pallas_call(functools.partial(layer_kernel, zs_n, ys_n, xs_n, cap), ou...]
where the time goes in v4:
time: 93.2 us; the launch traced here: 93 us
  Pallas kernels  91.5 us (98%)
  local copies, waits for them, and re-layouts  1.57 us (2%)
    pallas_call x1, Pallas kernels, on_device(): pl.pallas_call(functools.partial(layer_kernel, zs_n, ys_n, xs_n, cap), ou...  91.5 us

profile of v4, /device:TPU:1, one launch (start us, length us, event | category | flops | bytes accessed | tf_op | source)
XLA Modules:
  0.0 93.0 jit_solution(7147356933244920069)
XLA Ops:
  0.0 91.5 %routed_layer.1 = bf16[128,512]{1,0:T(8,128)(2,1)} custom-call(bf16[128,2048]{1,0:T(8,128)(2,1)} %tokens.1, f32[1,2048]{1,0:T(1,128)} %bitcast.5, s32[2,128]{1,0:T(2,128)} %bitcast.8, f32[2,128]{1,0:T(2,128)} %bitcast.9, f32[1,2048]{1,0:T(1,128)} %bitcast.6, bf16[16,128]{1,0:T(8,128)(2,1)} %b_in.1, bf16[16,128]{1,0:T(8,128)(2,1)} %bitcast.7, ...), custom_call_target="tpu_custom_call" | custom-call | tf_op jit(solution)/shard_map/routed_layer/pallas_call | solution.py:665
  91.5 1.6 %copy.12 = bf16[128,512]{1,0:T(8,128)(2,1)} copy(bf16[128,512]{1,0:T(8,128)(2,1)} %routed_layer.1) | data formatting | bytes 262144

commit v5 on v4

--- a/solution.py
+++ b/solution.py
@@ -34,6 +34,17 @@
     ys_n,
     xs_n,
     cap,
+    tokens_h,
+    gain_h,
+    routes_h,
+    scores_h,
+    bgate_h,
+    b_in_h,
+    b_out_h,
+    w_gate,
+    w_up,
+    w_down,
+    out,
     tokens,
     gain,
     routes_t,
@@ -41,10 +52,6 @@
     bgate,
     b_in,
     b_out,
-    w_gate,
-    w_up,
-    w_down,
-    out,
     normed,
     zsend,
     zrecv,
@@ -110,14 +117,16 @@
     rows_tok, width = tokens.shape
     dx = width // xs_n
     fx = w_gate.shape[2]
+    groups = return_groups(pairs)
+    lanes = 128
+    parts = dx // lanes
+    g_rows = [round_up(parts * len(g) * cap, 16) for g in groups]
+    g_low = [zs_n * sum(g_rows[:n]) for n in range(len(groups))]
     experts = zs_n * pairs
     arow = zsend.shape[2]
     slots = zs_n * arow
     erow = ysend.shape[1]
     far = hops.index(last)
-    groups = return_groups(pairs)
-    g_rows = [round_up(len(g) * cap, 16) for g in groups]
-    g_low = [zs_n * sum(g_rows[:n]) for n in range(len(groups))]
 
     def at(z_, y_, c_, x_):
         return ((z_ * ys_n + y_) * CORES + c_, x_)
@@ -144,6 +153,21 @@
     for dev in peers:
         pl.semaphore_signal(barrier, inc=1, device_id=dev, device_id_type=MESH_ID)
 
+    pairs_in = (
+        (tokens_h, tokens),
+        (routes_h, routes_t),
+        (gain_h, gain),
+        (b_in_h, b_in),
+        (b_out_h, b_out),
+        (bgate_h, bgate),
+        (scores_h, scores_t),
+    )
+    fetched = [
+        pltpu.make_async_copy(src, dst, local_sem.at[3 + n])
+        for n, (src, dst) in enumerate(pairs_in)
+    ]
+    for copy in fetched:
+        copy.start()
     weights = [
         pltpu.make_async_copy(w_gate.at[0], w_gu.at[:, pl.ds(0, fx)], local_sem.at[0]),
         pltpu.make_async_copy(w_up.at[0], w_gu.at[:, pl.ds(fx, fx)], local_sem.at[1]),
@@ -152,6 +176,8 @@
     for copy in weights:
         copy.start()
 
+    for copy in fetched:
+        copy.wait()
     tf = tokens[...].astype(f32)
     scaled = lax.rsqrt(jnp.sum(tf * tf, axis=-1, keepdims=True) * (1.0 / width) + NORM_EPSILON)
     nf = (tf * scaled * gain[...]).astype(bf16)
@@ -229,17 +255,17 @@
         pp = floor_div(q, erow)
         rem = q - pp * erow
         zz = floor_div(rem, cap)
-        return jnp.where(zz < zs_n, zz * step + pp * cap + (rem - zz * cap), -1.0)
+        return jnp.where(zz < zs_n, zz * step + pp * cap + (rem - zz * cap), -1e6)
 
     def permutation(rows, slots, step):
         q = lax.broadcasted_iota(jnp.int32, (rows, slots), 0).astype(f32)
         t = lax.broadcasted_iota(jnp.int32, (rows, slots), 1).astype(f32)
         return jnp.where(row_target(q, step) == t, 1.0, 0.0).astype(bf16)
 
-    def unpermutation(rows, slots, step):
+    def unpermutation(rows, slots, step, shift):
         q = lax.broadcasted_iota(jnp.int32, (slots, rows), 1).astype(f32)
         t = lax.broadcasted_iota(jnp.int32, (slots, rows), 0).astype(f32)
-        return jnp.where(row_target(q, step) == t, 1.0, 0.0).astype(bf16)
+        return jnp.where(row_target(q, step) + shift == t, 1.0, 0.0).astype(bf16)
 
     east, west = at(z, y, c, xpeer(1)), at(z, y, c, xpeer(xs_n - 1))
     partner = at(z, y, 1 - c, x)
@@ -459,7 +485,10 @@
     def z_return(n):
         group, step = groups[n], g_rows[n]
         many = len(group) * erow
-        perm = unpermutation(many, zs_n * step, step)
+        perms = [
+            unpermutation(many, zs_n * step, step, 1.0 * cc * len(group) * cap)
+            for cc in range(parts)
+        ]
         with jax.named_scope(f"back_wait{n}"):
             for i in group:
                 if i == last:
@@ -472,9 +501,11 @@
         moved = 0.0
         for hh in (0,) if group == [far] else (0, 1):
             rows = yback[group[0] : group[-1] + 1, hh].reshape(many, dx)
-            moved = moved + jnp.dot(perm, rows, preferred_element_type=f32)
+            for cc, perm in enumerate(perms):
+                piece = rows[:, cc * lanes : (cc + 1) * lanes]
+                moved = moved + jnp.dot(perm, piece, preferred_element_type=f32)
         base = sum(g_rows[:n])
-        zback[:, base : base + step] = moved.astype(bf16).reshape(zs_n, step, dx)
+        zback[:, base : base + step] = moved.astype(bf16).reshape(zs_n, step, lanes)
         rows = pl.ds(base, step)
         kept = []
         for r in near:
@@ -515,7 +546,7 @@
             copy.start()
             bx.append(copy)
 
-    order = ("d0", "d1", "n0", "m0", "d2", "n1", "m1", "n2", "b1", "m2", "planes", "b0", "c1", "b2", "e1", "c0", "c2", "o1", "e0", "f1", "e2", "g1", "f0", "o2", "f2", "e3", "i1", "g0", "core", "i0", "g2", "i2", "f3", "z0", "dense", "j2", "g3", "i3", "send", "z2", "z1")
+    order = ("d0", "d1", "n0", "m0", "d2", "n1", "m1", "n2", "b1", "m2", "planes", "b0", "c1", "b2", "e1", "c0", "c2", "o1", "e0", "f1", "e2", "g1", "f0", "o2", "f2", "e3", "i1", "g0", "core", "i0", "g2", "i2", "f3", "dense", "j2", "g3", "z0", "i3", "send", "z2", "z1")
     steps = dict(b=step_b, c=step_c, d=step_d, e=step_e, f=step_f, g=step_g, i=step_i, j=step_j)
     steps.update(m=step_m, n=step_n, o=step_o, z=z_return)
     others = dict(planes=branch_planes, core=branch_core, dense=branch_dense, send=branch_send)
@@ -531,17 +562,30 @@
         row = jnp.broadcast_to(sigmoid(d), sq)
         mixes.append(jnp.sum(jnp.where(sq_a == sq_b, row, 0.0), axis=1, keepdims=True))
 
-    def combine(n):
+    def column(row):
+        wide_row = jnp.broadcast_to(row, sq)
+        return jnp.sum(jnp.where(sq_a == sq_b, wide_row, 0.0), axis=1, keepdims=True)
+
+    spots = [column(come[r]) for r in (0, 1)]
+
+    def picks(n):
+        shape = (rows_tok, zs_n * g_rows[n])
+        t = lax.broadcasted_iota(jnp.int32, shape, 1).astype(f32) + 1.0 * g_low[n]
+        size = len(groups[n]) * cap
+        return [
+            [jnp.where(t == spots[r] + 1.0 * cc * size, 1.0, 0.0).astype(bf16) for cc in range(parts)]
+            for r in (0, 1)
+        ]
+
+    def combine(n, taken):
         base = sum(g_rows[:n])
-        shape = (zs_n * g_rows[n], rows_tok)
-        t = lax.broadcasted_iota(jnp.int32, shape, 0).astype(f32) + 1.0 * g_low[n]
-        rows = zgot[:, base : base + g_rows[n]].reshape(shape[0], dx)
-        total = None
-        for r in (0, 1):
-            g = jnp.where(t == come[r], 1.0, 0.0).astype(bf16)
-            term = lax.dot_general(g, rows, (((0,), (0,)), ((), ())), preferred_element_type=f32)
-            total = mixes[r] * term if total is None else total + mixes[r] * term
-        return total
+        rows = zgot[:, base : base + g_rows[n]].reshape(zs_n * g_rows[n], lanes)
+        terms = []
+        for cc in range(parts):
+            one = jnp.dot(taken[0][cc], rows, preferred_element_type=f32)
+            two = jnp.dot(taken[1][cc], rows, preferred_element_type=f32)
+            terms.append(mixes[0] * one + mixes[1] * two)
+        return jnp.concatenate(terms, axis=1)
 
     with jax.named_scope("bx_wait"):
         bx_all().wait_recv()
@@ -549,11 +593,12 @@
     for r in range(1, xs_n):
         share = share + bgot[r].astype(f32)
     share = share * branch_weight
-    for n, kept in returned:
+    for n, _ in returned:
+        taken = picks(n)
         with jax.named_scope(f"kept{n}"):
             if near:
                 zb_all(n).wait_recv()
-        share = share + combine(n)
+        share = share + combine(n, taken)
     out[...] = share.astype(out.dtype)
 
     with jax.named_scope("send_wait"):
@@ -604,12 +649,19 @@
     fg = expert_down.shape[1]
     arow = round_up(cap, 16)
     erow = round_up(zs_n * cap, 16)
-    back_rows = sum(round_up(len(g) * cap, 16) for g in return_groups(pairs))
+    back_rows = sum(round_up(dx // 128 * len(g) * cap, 16) for g in return_groups(pairs))
     bpart = branch_in.shape
     bf16, f32 = jnp.bfloat16, jnp.float32
     vm = lambda shape, dtype=bf16: pltpu.VMEM(shape, dtype)
     sem = lambda *shape: pltpu.SemaphoreType.DMA(shape)
     scratch = [
+        vm((rows_tok, width)),
+        vm((1, width), f32),
+        vm((2, rows_tok), jnp.int32),
+        vm((2, rows_tok), f32),
+        vm((1, width), f32),
+        vm(bpart),
+        vm(bpart),
         vm((rows_tok, width)),
         vm((pairs - 1, zs_n, arow, dx)),
         vm((pairs - 1, zs_n, arow, dx)),
@@ -627,12 +679,12 @@
         vm((erow, dx)),
         vm((ys_n, erow, dx)),
         vm((pairs, 2, erow, dx)),
-        vm((zs_n, back_rows, dx)),
-        vm((zs_n, back_rows, dx)),
+        vm((zs_n, back_rows, 128)),
+        vm((zs_n, back_rows, 128)),
         vm((2, zs_n, ys_n, CORES, *bpart)),
         vm((xs_n, rows_tok, dx)),
         vm((xs_n, rows_tok, dx)),
-        sem(3),
+        sem(10),
         sem(pairs),
         sem(pairs),
         sem(1),
@@ -665,7 +717,7 @@
     return pl.pallas_call(
         functools.partial(layer_kernel, zs_n, ys_n, xs_n, cap),
         out_shape=jax.ShapeDtypeStruct((rows_tok, dx), bf16),
-        in_specs=[in_vmem] * 7 + [in_hbm] * 3,
+        in_specs=[in_hbm] * 10,
         out_specs=in_vmem,
         scratch_shapes=scratch,
         compiler_params=pltpu.CompilerParams(

time: 93.2 us -> 88.9 us (0.954)
  Pallas kernels: 91.5 us -> 87 us
    pallas_call x1, Pallas kernels: 91.5 us -> 87 us  [on_device(): pl.pallas_call(functools.partial(layer_kernel, zs_n, ys_n, xs_n, cap), ou...]
where the time goes in v5:
time: 88.9 us; the launch traced here: 88.6 us
  Pallas kernels  87 us (98%)
  local copies, waits for them, and re-layouts  1.57 us (2%)
    pallas_call x1, Pallas kernels, on_device(): pl.pallas_call(functools.partial(layer_kernel, zs_n, ys_n, xs_n, cap), ou...  87 us

profile of v5, /device:TPU:1, one launch (start us, length us, event | category | flops | bytes accessed | tf_op | source)
XLA Modules:
  0.0 88.6 jit_solution(5078163888020599310)
XLA Ops:
  0.0 87.0 %routed_layer.1 = bf16[128,512]{1,0:T(8,128)(2,1)} custom-call(bf16[128,2048]{1,0:T(8,128)(2,1)} %tokens_h.1, f32[1,2048]{1,0:T(1,128)} %bitcast.5, s32[2,128]{1,0:T(2,128)} %bitcast.8, f32[2,128]{1,0:T(2,128)} %bitcast.9, f32[1,2048]{1,0:T(1,128)} %bitcast.6, bf16[16,128]{1,0:T(8,128)(2,1)} %b_in_h.1, bf16[16,128]{1,0:T(8,128)(2,1)} %bitcast.7, ...), custom_call_target="tpu_custom_call" | custom-call | tf_op jit(solution)/shard_map/routed_layer/pallas_call | solution.py:717
  87.0 1.6 %copy.12 = bf16[128,512]{1,0:T(8,128)(2,1)} copy(bf16[128,512]{1,0:T(8,128)(2,1)} %routed_layer.1) | data formatting | bytes 262144

commit v6 on v5

--- a/solution.py
+++ b/solution.py
@@ -65,6 +65,7 @@
     acc,
     psend,
     precv,
+    perms,
     half,
     qrecv,
     fsend,
@@ -204,11 +205,26 @@
             spot = low + zz * n_rows + (rel - group[0]) * cap
             place = spot if group[0] == 0 else jnp.where(rel > group[0] - 0.5, spot, place)
         come.append(rank + place)
-    srow = lax.broadcasted_iota(jnp.int32, (pairs * slots, rows_tok), 0).astype(f32)
-    pick = jnp.where((srow == go[0]) | (srow == go[1]), 1.0, 0.0).astype(bf16)
     own_cols = pl.ds(pl.multiple_of(x * dx, dx), dx)
-    packed = jnp.dot(pick[: last * slots], normed[:, own_cols], preferred_element_type=f32)
-    zsend[...] = packed.astype(bf16).reshape(last, zs_n, arow, dx)
+    wide_lanes = width // parts
+
+    def pack(i, source, n_lanes):
+        srow = lax.broadcasted_iota(jnp.int32, (slots, rows_tok), 0).astype(f32) + 1.0 * i * slots
+        total = 0.0
+        for cc in range(parts):
+            here = srow - 1.0 * cc * cap
+            pick = jnp.where((here == go[0]) | (here == go[1]), 1.0, 0.0).astype(bf16)
+            total = total + jnp.dot(pick, source(cc), preferred_element_type=f32)
+        return total.astype(bf16).reshape(zs_n, arow, n_lanes)
+
+    def narrow_source(cc):
+        start = pl.multiple_of(x * dx + cc * lanes, lanes)
+        return normed[:, pl.ds(start, lanes)]
+
+    def wide_source(cc):
+        return normed[:, cc * wide_lanes : (cc + 1) * wide_lanes]
+
+    zsend[0] = pack(0, narrow_source, lanes)
 
     pl.semaphore_wait(barrier, len(peers))
 
@@ -230,11 +246,10 @@
         return remote(ref, ref, zd_s.at[i], zd_r.at[i], at(z, y, 1 - c, x))
 
     z_send(0)
+    for i in range(1, last):
+        zsend[i] = pack(i, narrow_source, lanes)
     for i in range(last):
         zrecv[i, z] = zsend[i, z]
-    wide = jnp.dot(pick[last * slots :], normed[...], preferred_element_type=f32)
-    wsend[...] = wide.astype(bf16).reshape(zs_n, arow, width)
-    wrecv[z] = wsend[z]
     if near:
         zd_all(0).wait_send()
     z_send(1)
@@ -257,10 +272,15 @@
         zz = floor_div(rem, cap)
         return jnp.where(zz < zs_n, zz * step + pp * cap + (rem - zz * cap), -1e6)
 
-    def permutation(rows, slots, step):
+    def permutation(rows, slots, step, shift):
         q = lax.broadcasted_iota(jnp.int32, (rows, slots), 0).astype(f32)
         t = lax.broadcasted_iota(jnp.int32, (rows, slots), 1).astype(f32)
-        return jnp.where(row_target(q, step) == t, 1.0, 0.0).astype(bf16)
+        return jnp.where(row_target(q, step) + shift == t, 1.0, 0.0).astype(bf16)
+
+    for cc in range(parts):
+        perms[cc] = permutation(erow, slots, arow, 1.0 * cc * cap)
+    wsend[...] = pack(last, wide_source, wide_lanes)
+    wrecv[z] = wsend[z]
 
     def unpermutation(rows, slots, step, shift):
         q = lax.broadcasted_iota(jnp.int32, (slots, rows), 1).astype(f32)
@@ -311,17 +331,18 @@
         return (2 * i, 2 * i + 1)
 
     def step_d(i):
-        perm = permutation(erow, slots, arow)
         with jax.named_scope(f"z_wait{i}"):
             if near:
                 zd_all(i).wait_recv()
-        moved = jnp.dot(perm, zrecv[i].reshape(slots, dx), preferred_element_type=f32)
-        ysend[i] = moved.astype(bf16)
+        rows = zrecv[i].reshape(slots, lanes)
+        for cc in range(parts):
+            moved = jnp.dot(perms[cc], rows, preferred_element_type=f32)
+            ysend[i, :, cc * lanes : (cc + 1) * lanes] = moved.astype(bf16)
         pt = lax.rem(pair + pairs + offset[i] * (1 - 2 * h), pairs)
         near_chip = lax.rem(h + hops[i], 2)
         k = 2 * i + near_chip
         for n, hh in enumerate((near_chip, 1 - near_chip)):
-            if i == far and n == 1:
+            if hops[i] > 1 and n == 1:
                 break
             dst = tok.at[k, c, :, own_cols]
             dev = at(z, 2 * pt + hh, c, x)
@@ -335,12 +356,14 @@
     def step_o(part):
         mine = 2 * last + h
         if part == 1:
-            perm = permutation(erow, slots, arow)
             with jax.named_scope("z_wait_wide"):
                 if near:
                     zd_all(last).wait_recv()
-            moved = jnp.dot(perm, wrecv[...].reshape(slots, width), preferred_element_type=f32)
-            tok[mine, c] = moved.astype(bf16)
+            rows = wrecv[...].reshape(slots, wide_lanes)
+            for cc in range(parts):
+                moved = jnp.dot(perms[cc], rows, preferred_element_type=f32)
+                cols = slice(cc * wide_lanes, (cc + 1) * wide_lanes)
+                tok[mine, c, :, cols] = moved.astype(bf16)
             ref = tok.at[mine, c]
             begin(remote(ref, ref, yd_s.at[0], yd_r.at[mine], mate))
             to_partner(mine, ref)
@@ -375,7 +398,7 @@
         mine = 2 * i + h
         with jax.named_scope(f"n_wait{i}"):
             y_wait(mine)
-        if i == far:
+        if hops[i] > 1:
             ref = tok.at[mine, c, :, own_cols]
             begin(remote(ref, ref, yd_s.at[0], yd_r.at[mine], mate))
         spread(tok_part, tx_s, tx_r, mine)
@@ -437,7 +460,7 @@
             rows = hid[2 * i : 2 * i + 2].reshape(2 * CORES * erow, hid.shape[3])
             part = jnp.dot(rows, w_dn[...], preferred_element_type=f32)
             part = part.reshape(2, CORES, erow, dx)
-            acc[...] = part
+            acc[i] = part
             psend[2 * i : 2 * i + 2] = part.astype(bf16)
         two = pl.ds(2 * i, 2)
         pending["g", i] = begin(
@@ -447,7 +470,7 @@
     def step_i(i):
         with jax.named_scope(f"i_wait{i}"):
             pending["g", i].wait_recv()
-        total = acc[:, c] + precv[2 * i : 2 * i + 2].astype(f32)
+        total = acc[i, :, c] + precv[2 * i : 2 * i + 2].astype(f32)
         fsend[2 * i : 2 * i + 2] = total.astype(bf16)
         if i == last:
             yback[i, h] = fsend[2 * i + h]
@@ -546,7 +569,7 @@
             copy.start()
             bx.append(copy)
 
-    order = ("d0", "d1", "n0", "m0", "d2", "n1", "m1", "n2", "b1", "m2", "planes", "b0", "c1", "b2", "e1", "c0", "c2", "o1", "e0", "f1", "e2", "g1", "f0", "o2", "f2", "e3", "i1", "g0", "core", "i0", "g2", "i2", "f3", "dense", "j2", "g3", "z0", "i3", "send", "z2", "z1")
+    order = ("d0", "d1", "n0", "m0", "d2", "n1", "b0", "m1", "n2", "c0", "b1", "o1", "m2", "planes", "e0", "b2", "c1", "e1", "c2", "e2", "f1", "f0", "o2", "e3", "f2", "g1", "i1", "g2", "g0", "core", "i2", "i0", "f3", "dense", "j2", "g3", "i3", "z0", "send", "z2", "z1")
     steps = dict(b=step_b, c=step_c, d=step_d, e=step_e, f=step_f, g=step_g, i=step_i, j=step_j)
     steps.update(m=step_m, n=step_n, o=step_o, z=z_return)
     others = dict(planes=branch_planes, core=branch_core, dense=branch_dense, send=branch_send)
@@ -647,7 +670,7 @@
     dx = width // xs_n
     fx = expert_gate.shape[2]
     fg = expert_down.shape[1]
-    arow = round_up(cap, 16)
+    arow = round_up(dx // 128 * cap, 16)
     erow = round_up(zs_n * cap, 16)
     back_rows = sum(round_up(dx // 128 * len(g) * cap, 16) for g in return_groups(pairs))
     bpart = branch_in.shape
@@ -663,18 +686,19 @@
         vm(bpart),
         vm(bpart),
         vm((rows_tok, width)),
-        vm((pairs - 1, zs_n, arow, dx)),
-        vm((pairs - 1, zs_n, arow, dx)),
-        vm((zs_n, arow, width)),
-        vm((zs_n, arow, width)),
+        vm((pairs - 1, zs_n, arow, 128)),
+        vm((pairs - 1, zs_n, arow, 128)),
+        vm((zs_n, arow, width // (dx // 128))),
+        vm((zs_n, arow, width // (dx // 128))),
         vm((pairs - 1, erow, dx)),
         vm((ys_n, CORES, erow, width)),
         vm((width, 2 * fx)),
         vm((fg, dx)),
         vm((ys_n, CORES, erow, fg)),
-        vm((2, CORES, erow, dx), f32),
+        vm((pairs, 2, CORES, erow, dx), f32),
         vm((ys_n, CORES, erow, dx)),
         vm((ys_n, erow, dx)),
+        vm((dx // 128, erow, zs_n * arow)),
         vm((2, erow, dx), f32),
         vm((erow, dx)),
         vm((ys_n, erow, dx)),

time: 88.9 us -> 88.2 us (level)
  no operation moved by 1% of the time
where the time goes in v6:
time: 88.2 us; the launch traced here: 88.1 us
  Pallas kernels  86.5 us (98%)
  local copies, waits for them, and re-layouts  1.57 us (2%)
    pallas_call x1, Pallas kernels, on_device(): pl.pallas_call(functools.partial(layer_kernel, zs_n, ys_n, xs_n, cap), ou...  86.5 us

profile of v6, /device:TPU:1, one launch (start us, length us, event | category | flops | bytes accessed | tf_op | source)
XLA Modules:
  0.0 88.1 jit_solution(5092796929921428209)
XLA Ops:
  0.0 86.5 %routed_layer.1 = bf16[128,512]{1,0:T(8,128)(2,1)} custom-call(bf16[128,2048]{1,0:T(8,128)(2,1)} %tokens_h.1, f32[1,2048]{1,0:T(1,128)} %bitcast.5, s32[2,128]{1,0:T(2,128)} %bitcast.8, f32[2,128]{1,0:T(2,128)} %bitcast.9, f32[1,2048]{1,0:T(1,128)} %bitcast.6, bf16[16,128]{1,0:T(8,128)(2,1)} %b_in_h.1, bf16[16,128]{1,0:T(8,128)(2,1)} %bitcast.7, ...), custom_call_target="tpu_custom_call" | custom-call | tf_op jit(solution)/shard_map/routed_layer/pallas_call | solution.py:741
  86.5 1.6 %copy.12 = bf16[128,512]{1,0:T(8,128)(2,1)} copy(bf16[128,512]{1,0:T(8,128)(2,1)} %routed_layer.1) | data formatting | bytes 262144

commit v7 on v6

--- a/solution.py
+++ b/solution.py
@@ -569,7 +569,7 @@
             copy.start()
             bx.append(copy)
 
-    order = ("d0", "d1", "n0", "m0", "d2", "n1", "b0", "m1", "n2", "c0", "b1", "o1", "m2", "planes", "e0", "b2", "c1", "e1", "c2", "e2", "f1", "f0", "o2", "e3", "f2", "g1", "i1", "g2", "g0", "core", "i2", "i0", "f3", "dense", "j2", "g3", "i3", "z0", "send", "z2", "z1")
+    order = ("d0", "d1", "n0", "m0", "d2", "n1", "b0", "m1", "n2", "c0", "b1", "o1", "m2", "planes", "e0", "b2", "c1", "e1", "c2", "e2", "f1", "f0", "o2", "e3", "f2", "g1", "i1", "g2", "g0", "core", "i2", "i0", "f3", "dense", "j2", "g3", "z0", "i3", "send", "z2", "z1")
     steps = dict(b=step_b, c=step_c, d=step_d, e=step_e, f=step_f, g=step_g, i=step_i, j=step_j)
     steps.update(m=step_m, n=step_n, o=step_o, z=z_return)
     others = dict(planes=branch_planes, core=branch_core, dense=branch_dense, send=branch_send)

time: 88.2 us -> 87.3 us (0.990)
  Pallas kernels: 86.5 us -> 85.3 us
    pallas_call x1, Pallas kernels: 86.5 us -> 85.3 us  [on_device(): pl.pallas_call(functools.partial(layer_kernel, zs_n, ys_n, xs_n, cap), ou...]
where the time goes in v7:
time: 87.3 us; the launch traced here: 86.9 us
  Pallas kernels  85.3 us (98%)
  local copies, waits for them, and re-layouts  1.57 us (2%)
    pallas_call x1, Pallas kernels, on_device(): pl.pallas_call(functools.partial(layer_kernel, zs_n, ys_n, xs_n, cap), ou...  85.3 us

profile of v7, /device:TPU:1, one launch (start us, length us, event | category | flops | bytes accessed | tf_op | source)
XLA Modules:
  0.0 86.9 jit_solution(2757171987824167084)
XLA Ops:
  0.0 85.3 %routed_layer.1 = bf16[128,512]{1,0:T(8,128)(2,1)} custom-call(bf16[128,2048]{1,0:T(8,128)(2,1)} %tokens_h.1, f32[1,2048]{1,0:T(1,128)} %bitcast.5, s32[2,128]{1,0:T(2,128)} %bitcast.8, f32[2,128]{1,0:T(2,128)} %bitcast.9, f32[1,2048]{1,0:T(1,128)} %bitcast.6, bf16[16,128]{1,0:T(8,128)(2,1)} %b_in_h.1, bf16[16,128]{1,0:T(8,128)(2,1)} %bitcast.7, ...), custom_call_target="tpu_custom_call" | custom-call | tf_op jit(solution)/shard_map/routed_layer/pallas_call | solution.py:741
  85.3 1.6 %copy.12 = bf16[128,512]{1,0:T(8,128)(2,1)} copy(bf16[128,512]{1,0:T(8,128)(2,1)} %routed_layer.1) | data formatting | bytes 262144
